TPU v7x, 256 devices: a whole 4x4x8 slice. The times are simulated.
256 devices in a mesh: ep: 16 (over y, x), tp: 16 (over z, core).
Axes of the slice: x: 4, y: 4, z: 8, core: 2. Of those that a mesh axis runs over, the one named last changes fastest.
Arguments:
- query_heads_rows: bfloat16 [8192, 2048], P('ep', 'tp'), may hold values from -9 to 9
- key_heads_rows: bfloat16 [8192, 2048], P('ep', 'tp'), may hold values from -9 to 9
- value_heads_rows: bfloat16 [8192, 2048], P('ep', 'tp'), may hold values from -6 to 6
- write_strength_logit: bfloat16 [16, 8192], P('tp', 'ep'), may hold values from -3.5 to -1
- decay_preactivation: bfloat16 [16, 8192], P('tp', 'ep'), may hold values from -5 to 5
- head_decay_logarithm: float32 [16], P('tp'), may hold values from -20 to -3
- extra_log_decay: float32 [16, 8192], P('tp', 'ep'), may hold values from -0.7 to 0
- output_weight: bfloat16 [2048, 2048], P('tp'), may hold values from -2 to 2
- second_batch_tokens: bfloat16 [32768, 2048], P(('ep', 'tp')), may hold values from -6 to 6
- expert_norm_scale: float32 [2048], replicated, may hold values from 0.1 to 1.9
- expert_choice_index: int32 [32768, 2], P(('ep', 'tp')), may hold values from 0 to 15, as said below
- group_router_weight: float32 [32768], P(('ep', 'tp')), may hold values from 0.25 to 1
- expert_logit_difference: float32 [32768], P(('ep', 'tp')), may hold values from -8 to 8
- expert_gate_weight: bfloat16 [16, 1024, 2048], P('ep', 'tp'), may hold values from -0.125 to 0.125
- expert_up_weight: bfloat16 [16, 1024, 2048], P('ep', 'tp'), may hold values from -0.125 to 0.125
- expert_down_weight: bfloat16 [16, 1024, 2048], P('ep', 'tp'), may hold values from -0.375 to 0.375
Outputs:
- mixer_output_first: bfloat16 [8192, 2048], P(('ep', 'tp'))
- expert_out: bfloat16 [32768, 2048], P(('ep', 'tp'))
Inputs may be any that keep to these rules, and one draw needn't show every extreme that they name: `expert_choice_index`: each row names two different experts of one group, the experts a * 4 to a * 4 + 3 for some a. In the rows of one device (aligned blocks of 128 rows) no expert is named more than 32 times, and in every device's rows some expert is named exactly 32 times.
All inputs are finite; a program needn't handle non-finite values.
Results may differ from a plain program's by a relative error of at most 0.018.
Values may be sent and summed in bfloat16 or wider, within the bound.
A program may use at most 64 MiB of HBM per device.

v0:
```python
import jax
import jax.numpy as jnp
from jax import lax
from jax.sharding import Mesh
from jax.sharding import PartitionSpec as P

DK = 128
DV = 128
BLOCK = 64
CAP = 32
EXPERTS = 16
TOPK = 2
EP = ("ep_0", "ep_1")
EP_TP = ("ep_0", "ep_1", "tp")


norm_eps = 1e-06


def filled_with(value, identity):
    return jax.tree.map(
        lambda part, zero: jnp.zeros_like(part) + jnp.asarray(zero, part.dtype), value, identity
    )


def entering(value, axes, combine, identity):
    before = start = filled_with(value, identity)
    subtotal = value
    for axis in reversed(axes):
        peers, here = (lax.axis_size(axis), lax.axis_index(axis))
        pieces = jax.tree.map(lambda part: lax.all_gather(part, axis), subtotal)
        inside, subtotal = (start, start)
        for k in range(peers):
            passed = k < here
            subtotal = combine(subtotal, jax.tree.map(lambda part: part[k], pieces))
            inside = jax.tree.map(lambda new, old: jnp.where(passed, new, old), subtotal, inside)
        before = combine(inside, before)
    return before


def in_blocks(value, dim, peers):
    before, after = (value.shape[:dim], value.shape[dim + 1 :])
    return jnp.moveaxis(value.reshape(*before, peers, -1, *after), dim, 0)


def cut_rows(length, count):
    unit = 8 if length >= 8 * count else 1
    return [length // unit * k // count * unit for k in range(1, count)]


def in_order(parts, dim):
    dims = list(parts.shape[1:])
    dims[dim] *= parts.shape[0]
    return jnp.moveaxis(parts, 0, dim).reshape(dims)


def exchange_in_pieces(value, axis, pieces, split_dim, concat_dim):
    parts = in_blocks(value, split_dim, lax.axis_size(axis))
    split_at = max(range(1, max(2, parts.ndim - 1)), key=lambda d: parts.shape[d])
    done = []
    for section in jnp.split(parts, cut_rows(parts.shape[split_at], pieces), axis=split_at):
        if section.size:
            done.append(lax.all_to_all(section, axis, split_axis=0, concat_axis=0, tiled=True))
    return in_order(jnp.concatenate(done, axis=split_at), concat_dim)


def in_one_piece(arrays, axis, dim, along):
    widths = [a.shape[along] for a in arrays]
    both = jnp.concatenate(arrays, axis=along)
    filled = lax.all_gather(both, axis, axis=dim, tiled=True)
    return tuple(jnp.split(filled, [sum(widths[:k]) for k in range(1, len(widths))], axis=along))


def unit_rows(matrix):
    return matrix * lax.rsqrt(jnp.sum(matrix * matrix, axis=-1, keepdims=True) + norm_eps)


def block_terms(query_block, key_block, value_block, decay_logarithm, strength):
    span_len = query_block.shape[2]
    dim_value = value_block.shape[-1]
    cumulative = jnp.cumsum(decay_logarithm, axis=-1)
    within = jnp.tril(jnp.ones((span_len, span_len), bool))
    strict = jnp.tril(jnp.ones((span_len, span_len), bool), -1)
    spread = cumulative[..., :, None] - cumulative[..., None, :]
    decayed = jnp.where(within, jnp.exp(jnp.where(within, spread, 0.0)), 0.0)
    weighted = key_block * strength[..., None]
    lower_part = jnp.where(
        strict, jnp.einsum("hnid,hnjd->hnij", weighted, key_block) * decayed, 0.0
    )
    system = lower_part + jnp.eye(span_len, dtype=jnp.float32)
    rhs_cols = jnp.concatenate(
        [value_block * strength[..., None], weighted * jnp.exp(cumulative)[..., None]], axis=-1
    )
    solved = jax.scipy.linalg.solve_triangular(system, rhs_cols, lower=True, unit_diagonal=True)
    updated_values = solved[..., :dim_value]
    delta_corrections = solved[..., dim_value:]
    scores = jnp.where(within, jnp.einsum("hnid,hnjd->hnij", query_block, key_block) * decayed, 0.0)
    decayed_queries = query_block * jnp.exp(cumulative)[..., None]
    decayed_keys = key_block * jnp.exp(cumulative[..., -1:] - cumulative)[..., None]
    block_retention = jnp.exp(cumulative[..., -1])
    return (
        decayed_queries,
        decayed_keys,
        updated_values,
        delta_corrections,
        scores,
        block_retention,
    )


def carry_step(recurrent_state, inputs):
    decayed_queries, decayed_keys, updated_values, delta_corrections, scores, block_retention = (
        inputs
    )
    value_updates = updated_values - jnp.einsum("jdb,jbu->jdu", delta_corrections, recurrent_state)
    final_output = jnp.einsum("jdb,jbu->jdu", decayed_queries, recurrent_state)
    final_output = final_output + jnp.einsum("hcj,hjv->hcv", scores, value_updates)
    recurrent_state = recurrent_state * block_retention[:, None, None] + jnp.einsum(
        "rpq,rpd->rqd", decayed_keys, value_updates
    )
    return (recurrent_state, final_output)


def compose(earlier, latter):
    joined_map = jnp.einsum("hij,hjk->hik", latter[0], earlier[0])
    joined_state = jnp.einsum("hij,hjv->hiv", latter[0], earlier[1]) + latter[1]
    return (joined_map, joined_state)


def shards(
    query_heads_rows,
    key_heads_rows,
    value_heads_rows,
    write_strength_logit,
    decay_preactivation,
    head_decay_logarithm,
    extra_log_decay,
    output_weight,
    second_batch_tokens,
    expert_norm_scale,
    expert_choice_index,
    group_router_weight,
    expert_logit_difference,
    expert_gate_weight,
    expert_up_weight,
    expert_down_weight,
):
    length = query_heads_rows.shape[0]
    local_heads = head_decay_logarithm.shape[0]
    blocks = length // BLOCK
    width_model = output_weight.shape[1]

    def heads_first(matrix):
        spread_out = matrix.astype(jnp.float32).reshape(length, local_heads, -1).transpose(1, 0, 2)
        return spread_out.reshape(local_heads, blocks, BLOCK, -1)

    query_block = unit_rows(heads_first(query_heads_rows)) * DK ** (-0.5)
    key_block = unit_rows(heads_first(key_heads_rows))
    value_block = heads_first(value_heads_rows)
    strength = jax.nn.sigmoid(write_strength_logit.astype(jnp.float32)).reshape(
        local_heads, blocks, BLOCK
    )
    decay_logarithm = (
        -jnp.exp(head_decay_logarithm)[:, None]
        * jax.nn.softplus(decay_preactivation.astype(jnp.float32))
        + extra_log_decay
    )
    decay_logarithm = decay_logarithm.reshape(local_heads, blocks, BLOCK)
    decayed_queries, decayed_keys, updated_values, delta_corrections, scores, block_retention = (
        block_terms(query_block, key_block, value_block, decay_logarithm, strength)
    )
    fresh_wide = jnp.concatenate(
        [updated_values, jnp.zeros(updated_values.shape[:-1] + (DK,), jnp.float32)], axis=-1
    )
    inputs = tuple(
        (
            jnp.moveaxis(term, 1, 0)
            for term in (
                decayed_queries,
                decayed_keys,
                fresh_wide,
                delta_corrections,
                scores,
                block_retention,
            )
        )
    )
    identity_map = jnp.broadcast_to(jnp.eye(DK, dtype=jnp.float32), (local_heads, DK, DK))
    start_memory = jnp.concatenate(
        [jnp.zeros((local_heads, DK, DV), jnp.float32), identity_map], axis=-1
    )
    end_memory, outputs = lax.scan(carry_step, start_memory, inputs)
    local_output = outputs[..., :DV]
    projection_matrix = outputs[..., DV:]
    carried_end = end_memory[..., :DV]
    transfer = end_memory[..., DV:]
    _, incoming_rows = entering(
        (transfer, carried_end), EP, compose, (identity_map, jnp.zeros_like(carried_end))
    )
    attention_result = local_output + jnp.einsum("xtyg,tgd->xtyd", projection_matrix, incoming_rows)
    attn_rows = (
        attention_result.transpose(0, 2, 1, 3)
        .reshape(length, local_heads * DV)
        .astype(jnp.bfloat16)
    )
    summed = lax.psum_scatter(
        jnp.dot(attn_rows, output_weight, preferred_element_type=jnp.float32).astype(jnp.bfloat16),
        "tp",
        scatter_dimension=0,
        tiled=True,
    )
    widened = second_batch_tokens.astype(jnp.float32)
    normed = (
        widened
        * lax.rsqrt(jnp.mean(widened * widened, axis=-1, keepdims=True) + norm_eps)
        * expert_norm_scale
    ).astype(jnp.bfloat16)
    own_tokens = second_batch_tokens.shape[0]
    ep_count = lax.axis_size(EP)
    local_experts = EXPERTS // ep_count
    flat_ids = expert_choice_index.reshape(-1)
    one_hot = (flat_ids[:, None] == jnp.arange(EXPERTS, dtype=jnp.int32)[None, :]).astype(jnp.int32)
    slot_rank = jnp.sum((jnp.cumsum(one_hot, axis=0) - one_hot) * one_hot, axis=1)
    slot_index = flat_ids * CAP + slot_rank
    copy_token = jnp.arange(flat_ids.shape[0], dtype=jnp.int32) // TOPK
    slot_token = jnp.full((EXPERTS * CAP,), own_tokens, jnp.int32).at[slot_index].set(copy_token)
    outgoing = jnp.take(normed, slot_token, axis=0, mode="fill", fill_value=0).reshape(
        ep_count, local_experts, CAP, width_model
    )
    arrived = exchange_in_pieces(outgoing, EP, 2, 0, 0)
    gate_piece, up_piece, down_piece = in_one_piece(
        (expert_gate_weight, expert_up_weight, expert_down_weight), "tp", 1, 0
    )
    gating = jnp.einsum("secd,efd->secf", arrived, gate_piece, preferred_element_type=jnp.float32)
    upward = jnp.einsum("secd,efd->secf", arrived, up_piece, preferred_element_type=jnp.float32)
    hidden = (jax.nn.silu(gating) * upward).astype(jnp.bfloat16)
    produced = jnp.einsum("secf,efd->secd", hidden, down_piece, preferred_element_type=jnp.float32)
    returned = lax.all_to_all(
        produced.astype(jnp.bfloat16), EP, split_axis=0, concat_axis=0, tiled=True
    )
    flat_results = returned.reshape(EXPERTS * CAP, width_model)
    picked = (
        jnp.take(flat_results, slot_index, axis=0)
        .reshape(own_tokens, TOPK, width_model)
        .astype(jnp.float32)
    )
    leading = jax.nn.sigmoid(expert_logit_difference)
    mixing = group_router_weight[:, None] * jnp.stack([leading, 1.0 - leading], axis=-1)
    expert_out = jnp.sum(mixing[..., None] * picked, axis=1).astype(jnp.bfloat16)
    return (summed, expert_out)


def solution(mesh):
    split = Mesh(mesh.devices.reshape(4, 4, mesh.shape["tp"]), ("ep_0", "ep_1", "tp"))
    placed = (
        P(EP, "tp"),
        P(EP, "tp"),
        P(EP, "tp"),
        P("tp", EP),
        P("tp", EP),
        P("tp"),
        P("tp", EP),
        P("tp", None),
        P(EP_TP, None),
        P(),
        P(EP_TP, None),
        P(EP_TP),
        P(EP_TP),
        P(EP, "tp", None),
        P(EP, "tp", None),
        P(EP, "tp", None),
    )
    return jax.shard_map(
        shards,
        mesh=split,
        in_specs=placed,
        out_specs=(P(EP_TP, None), P(EP_TP, None)),
        check_vma=False,
    )
```

profile of v0, /device:TPU:1, one launch (start us, length us, event | category | flops | bytes accessed | tf_op | source)
XLA Modules:
  0.0 220.0 jit_solution(6963558183725057026)
XLA Ops:
  7.3 2.2 pad_maximum_fusion
  9.9 0.6 reduce-window.6
  11.1 1.4 scatter_custom_fusion
  13.0 2.5 %gather_fusion = bf16[512,2048]{1,0:T(8,128)(2,1)S(1)} fusion(bf16[128,2048]{1,0:T(8,128)(2,1)S(1)} %fusion.44, s32[1024]{0:T(1024)S(1)} %pad_clamp_fusion.1), kind=kCustom, calls=%fused_computation | custom fusion | bytes 4196352 | tf_op jit(solution)/shard_map/jit(_take)/gather | solution.py:227
  15.7 1.5 fusion.137
  17.2 7.7 %all-to-all-start = ((bf16[16,1,1,16,2048]{4,3,2,1,0:T(8,128)(2,1)}), bf16[16,1,1,16,2048]{4,3,2,1,0:T(8,128)(2,1)S(1)}, u32[]{:S(2)}, u32[]{:S(2)}) async-start(bf16[16,1,1,16,2048]{4,3,2,1,0:T(8,128)(2,1)} %get-tuple-element.110), calls=%async_computation.1 | async-start | bytes 2097152 | tf_op jit(solution)/shard_map/all_to_all | solution.py:63
  26.9 39.3 %custom-call.4 = f32[8,1,64,64]{2,3,1,0:T(8,128)S(1)} custom-call(f32[8,1,64,64]{3,2,1,0:T(8,128)S(1)} %fusion.35), custom_call_target="InvertDiagBlocksLowerTriangular" | custom-call | tf_op jit(solution)/shard_map/jit(_solve_triangular)/vmap()/triangular_solve | solution.py:94
  67.4 0.6 fusion.45
  68.6 19.5 %while.12 = (s32[]{:T(128)}, f32[1,128,256]{2,1,0:T(8,128)S(1)}, f32[8,1,64,256]{3,2,1,0:T(8,128)}, f32[8,1]{0,1:T(1,128)S(1)}, bf16[8,1,64,128]{3,2,1,0:T(8,128...) while((s32[]{:T(128)}, f32[1,128,256]{2,1,0:T(8,128)S(1)}, ...), condition=%wide.region_4.5_spmd, body=%wide.region_3.4_spmd.sunk | while | flops 14794754 | bytes 952445 | solution.py:192
  68.9 0.8 fusion.181
  69.7 0.6 constant_dynamic-slice_fusion.2
  70.2 0.8 fusion.179
  71.3 0.8 fusion.181
  72.1 0.6 constant_dynamic-slice_fusion.2
  72.7 0.8 fusion.179
  73.8 0.8 fusion.181
  74.5 0.6 constant_dynamic-slice_fusion.2
  75.1 0.8 fusion.179
  76.2 0.8 fusion.181
  77.0 0.6 constant_dynamic-slice_fusion.2
  77.5 0.8 fusion.179
  78.6 0.8 fusion.181
  79.4 0.6 constant_dynamic-slice_fusion.2
  80.0 0.8 fusion.179
  81.1 0.8 fusion.181
  81.8 0.6 constant_dynamic-slice_fusion.2
  82.4 0.8 fusion.179
  83.5 0.8 fusion.181
  84.8 0.8 fusion.179
  85.9 0.8 fusion.181
  86.7 0.6 constant_dynamic-slice_fusion.2
  87.3 0.8 fusion.179
  88.1 9.9 %all-gather = bf16[4,128,128]{2,1,0:T(8,128)(2,1)S(1)} all-gather(bf16[1,128,128]{2,1,0:T(8,128)(2,1)S(1)} %slice.84), channel_id=2, replica_groups=mesh['ep_0'=4,'ep_1'=4,'tp'=16] {'ep_1'}, dimensions={0}, use_global_device_ids=true | all-gather | bytes 163840 | tf_op jit(solution)/shard_map/all_gather | solution.py:31
  98.6 9.4 %all-gather.1 = bf16[512,128]{1,0:T(8,128)(2,1)S(1)} all-gather(bf16[128,128]{1,0:T(8,128)(2,1)S(1)} %fusion.87), channel_id=3, replica_groups=mesh['ep_0'=4,'ep_1'=4,'tp'=16] {'ep_0'}, dimensions={0}, use_global_device_ids=true | all-gather | bytes 163840 | tf_op jit(solution)/shard_map/all_gather | solution.py:31
  108.0 9.7 %all-gather.2 = f32[4,128,128]{2,1,0:T(8,128)S(1)} all-gather(f32[1,128,128]{2,1,0:T(8,128)S(1)} %slice.93), channel_id=4, replica_groups=mesh['ep_0'=4,'ep_1'=4,'tp'=16] {'ep_1'}, dimensions={0}, use_global_device_ids=true | all-gather | bytes 327680 | tf_op jit(solution)/shard_map/all_gather | solution.py:31
  118.2 9.4 %all-gather.3 = f32[512,128]{1,0:T(8,128)S(1)} all-gather(f32[128,128]{1,0:T(8,128)S(1)} %convolution_add_fusion.5), channel_id=5, replica_groups=mesh['ep_0'=4,'ep_1'=4,'tp'=16] {'ep_0'}, dimensions={0}, use_global_device_ids=true | all-gather | bytes 327680 | tf_op jit(solution)/shard_map/all_gather | solution.py:31
  127.9 5.2 %all-to-all-start.1 = ((bf16[16,1,1,16,2048]{4,3,2,1,0:T(8,128)(2,1)}), bf16[16,1,1,16,2048]{4,3,2,1,0:T(8,128)(2,1)S(1)}, u32[]{:S(2)}, u32[]{:S(2)}) async-start(bf16[16,1,1,16,2048]{4,3,2,1,0:T(8,128)(2,1)} %get-tuple-element.111), calls=%async_computation.2 | async-start | bytes 2097152 | tf_op jit(solution)/shard_map/all_to_all | solution.py:63
  133.8 1.4 fusion.36
  135.2 2.1 convolution_convert_fusion
  137.2 8.1 %all-to-all-done.1 = bf16[16,1,1,16,2048]{4,3,2,1,0:T(8,128)(2,1)S(1)} async-done(((bf16[16,1,1,16,2048]{4,3,2,1,0:T(8,128)(2,1)}), bf16[16,1,1,16,2048]{4,3,2,1,0:T(8,128)(2,1)S(1)}, u32[]{:S(2)}, u32[]{:S(2)}) %all-to-all-start.1) | async-done | bytes 1048608 | tf_op jit(solution)/shard_map/all_to_all | solution.py:63
  145.3 5.9 %fusion.18 = f32[1024,16,32]{0,2,1:T(8,128)} fusion(bf16[3,1024,2048]{2,1,0:T(8,128)(2,1)} %all-gather.6.cloned.1.call-done, bf16[16,1,1,16,2048]{4,3,0,2,1:T(8,128)(2,1)S(1)} %bitcast.289, bf16[16,1,1,16,2048]{4,3,0,2,1:T(8,128)(2,1)S(1)} %bitcast.287), kind=kOutput, calls=%fused_computation.26 | convolution fusion | flops 2151677952 | bytes 8388608 | tf_op jit(solution)/shard_map/secd,efd->secf/dot_general | solution.py:235
  151.2 10.0 %fusion.22 = bf16[16,1,32,2048]{3,2,1,0:T(8,128)(2,1)} fusion(bf16[3,1024,2048]{2,1,0:T(8,128)(2,1)} %all-gather.6.cloned.1.call-done, f32[1024,16,32]{0,2,1:T(8,128)} %fusion.18, bf16[16,1,1,16,2048]{4,3,0,2,1:T(8,128)(2,1)S(1)} %bitcast.290, bf16[16,1,1,16,2048]{4,3,0,2,1:T(8,128)(2,1)S(1)} %bitcast.288), kind=kOutput, calls=%fused_computation.33 | convolution fusion | flops 4303355904 | bytes 14680064 | tf_op jit(solution)/shard_map/secf,efd->secd/dot_general | solution.py:237
  161.3 3.8 %all-to-all-start.2 = ((bf16[16,1,32,2048]{3,2,1,0:T(8,128)(2,1)}), bf16[16,1,32,2048]{3,2,1,0:T(8,128)(2,1)S(1)}, u32[]{:S(2)}, u32[]{:S(2)}) async-start(bf16[16,1,32,2048]{3,2,1,0:T(8,128)(2,1)} %fusion.22), calls=%async_computation.3 | async-start | bytes 4194304 | tf_op jit(solution)/shard_map/all_to_all | solution.py:238
  165.7 19.2 %all-to-all-done.2 = bf16[16,1,32,2048]{3,2,1,0:T(8,128)(2,1)S(1)} async-done(((bf16[16,1,32,2048]{3,2,1,0:T(8,128)(2,1)}), bf16[16,1,32,2048]{3,2,1,0:T(8,128)(2,1)S(1)}, u32[]{:S(2)}, u32[]{:S(2)}) %all-to-all-start.2) | async-done | bytes 2097184 | tf_op jit(solution)/shard_map/all_to_all | solution.py:238
  184.9 2.3 %gather_fusion.1 = bf16[256,2048]{1,0:T(8,128)(2,1)} fusion(bf16[512,2048]{1,0:T(8,128)(2,1)S(1)} %bitcast.280, s32[1024]{0:T(1024)S(1)} %pad_clamp_fusion), kind=kCustom, calls=%fused_computation.1 | custom fusion | bytes 2098176 | tf_op jit(solution)/shard_map/jit(_take)/gather | solution.py:243
  187.3 1.7 gather.15
  189.0 4.9 %multiply_reduce_fusion = bf16[128,2048]{1,0:T(8,128)(2,1)} fusion(bf16[128,2,2048]{2,1,0:T(2,128)(2,1)S(1)} %gather.15, pred[128,2]{1,0:T(8,128)(4,1)S(1)} %copy.63, f32[128,2]{1,0:T(8,128)S(1)} %copy.58), kind=kLoop, calls=%fused_computation.42 | loop fusion | flops 1835008 | bytes 1574144 | tf_op jit(solution)/shard_map/reduce_sum | solution.py:249
  193.9 19.2 %reduce-scatter.2.cloned.1.call-done = bf16[32,2048]{1,0:T(8,128)(2,1)} async-done(((bf16[512,2048]{1,0:T(8,128)(2,1)}), bf16[32,2048]{1,0:T(8,128)(2,1)}) %reduce-scatter.2.cloned.1.call-update) | async-done | bytes 131088 | tf_op jit(solution)/shard_map/reduce_scatter | solution.py:206
  (119 shorter events, 9.8 us)
Async XLA Ops:
  7.2 128.0 %copy-start = (bf16[128,2048]{1,0:T(8,128)(2,1)S(1)}, bf16[128,2048]{1,0:T(8,128)(2,1)}, u32[]{:S(2)}) copy-start(bf16[128,2048]{1,0:T(8,128)(2,1)} %param.25) | copy-start | bytes 1572868
  7.2 2.3 %copy-start.5 = (s32[128,2]{0,1:T(2,128)S(1)}, s32[128,2]{0,1:T(2,128)}, u32[]{:S(2)}) copy-start(s32[128,2]{0,1:T(2,128)} %param.28) | copy-start | bytes 3076
  7.2 5.4 %copy-start.1 = (bf16[128,2048]{1,0:T(8,128)(2,1)S(1)}, bf16[128,2048]{1,0:T(8,128)(2,1)}, u32[]{:S(2)}) copy-start(bf16[128,2048]{1,0:T(8,128)(2,1)} %param.26) | copy-start | bytes 1572868
  7.2 5.6 %copy-start.6 = (f32[2048]{0:T(1024)S(1)}, f32[2048]{0:T(1024)}, u32[]{:S(2)}) copy-start(f32[2048]{0:T(1024)} %param.27) | copy-start | bytes 24580
  7.2 138.1 %all-gather.6.cloned.1.call-start = ((), (), s32[]{:S(2)}) async-start(), calls=%async_computation.5 | async-start | bytes 13369344 | tf_op jit(solution)/shard_map/all_gather | solution.py:70
  17.2 8.5 %copy-start.7 = (bf16[1,512]{1,0:T(2,128)(2,1)S(1)}, bf16[1,512]{1,0:T(2,128)(2,1)}, u32[]{:S(2)}) copy-start(bf16[1,512]{1,0:T(2,128)(2,1)} %param.21) | copy-start | bytes 3076
  17.2 8.5 %copy-start.8 = (f32[1,512]{1,0:T(1,128)S(1)}, f32[1,512]{1,0:T(1,128)}, u32[]{:S(2)}) copy-start(f32[1,512]{1,0:T(1,128)} %param.24) | copy-start | bytes 6148
  17.2 8.5 %copy-start.9 = (bf16[1,512]{1,0:T(2,128)(2,1)S(1)}, bf16[1,512]{1,0:T(2,128)(2,1)}, u32[]{:S(2)}) copy-start(bf16[1,512]{1,0:T(2,128)(2,1)} %param.22) | copy-start | bytes 3076
  17.2 8.6 %copy-start.2 = (bf16[512,128]{1,0:T(8,128)(2,1)S(1)}, bf16[512,128]{1,0:T(8,128)(2,1)}, u32[]{:S(2)}) copy-start(bf16[512,128]{1,0:T(8,128)(2,1)} %param.19) | copy-start | bytes 393220
  17.2 49.0 %copy-start.3 = (bf16[512,128]{1,0:T(8,128)(2,1)S(1)}, bf16[512,128]{1,0:T(8,128)(2,1)}, u32[]{:S(2)}) copy-start(bf16[512,128]{1,0:T(8,128)(2,1)} %param.18) | copy-start | bytes 393220
  17.2 110.7 %all-to-all-start = ((bf16[16,1,1,16,2048]{4,3,2,1,0:T(8,128)(2,1)}), bf16[16,1,1,16,2048]{4,3,2,1,0:T(8,128)(2,1)S(1)}, u32[]{:S(2)}, u32[]{:S(2)}) async-start(bf16[16,1,1,16,2048]{4,3,2,1,0:T(8,128)(2,1)} %get-tuple-element.110), calls=%async_computation.1 | async-start | bytes 2097152 | tf_op jit(solution)/shard_map/all_to_all | solution.py:63
  24.9 42.2 %copy-start.4 = (bf16[512,128]{1,0:T(8,128)(2,1)S(1)}, bf16[512,128]{1,0:T(8,128)(2,1)}, u32[]{:S(2)}) copy-start(bf16[512,128]{1,0:T(8,128)(2,1)} %param.20) | copy-start | bytes 393220
  66.7 1.8 copy-start.10
  127.9 17.4 %all-to-all-start.1 = ((bf16[16,1,1,16,2048]{4,3,2,1,0:T(8,128)(2,1)}), bf16[16,1,1,16,2048]{4,3,2,1,0:T(8,128)(2,1)S(1)}, u32[]{:S(2)}, u32[]{:S(2)}) async-start(bf16[16,1,1,16,2048]{4,3,2,1,0:T(8,128)(2,1)} %get-tuple-element.111), calls=%async_computation.2 | async-start | bytes 2097152 | tf_op jit(solution)/shard_map/all_to_all | solution.py:63
  133.1 80.0 %reduce-scatter.2.cloned.1.call-start = ((), (), s32[]{:S(2)}) async-start(), calls=%async_computation.4 | async-start | bytes 2228224 | tf_op jit(solution)/shard_map/reduce_scatter | solution.py:206
  161.3 4.2 %copy-start.12 = (f32[128]{0:T(128)S(1)}, f32[128]{0:T(128)}, u32[]{:S(2)}) copy-start(f32[128]{0:T(128)} %param.30) | copy-start | bytes 1540
  161.3 4.3 %copy-start.11 = (f32[128]{0:T(128)S(1)}, f32[128]{0:T(128)}, u32[]{:S(2)}) copy-start(f32[128]{0:T(128)} %param.29) | copy-start | bytes 1540
  161.3 23.6 %all-to-all-start.2 = ((bf16[16,1,32,2048]{3,2,1,0:T(8,128)(2,1)}), bf16[16,1,32,2048]{3,2,1,0:T(8,128)(2,1)S(1)}, u32[]{:S(2)}, u32[]{:S(2)}) async-start(bf16[16,1,32,2048]{3,2,1,0:T(8,128)(2,1)} %fusion.22), calls=%async_computation.3 | async-start | bytes 4194304 | tf_op jit(solution)/shard_map/all_to_all | solution.py:238
Sparse Core Ops, SparseCore 0:
  9.9 79.8 all-gather.5
  137.4 75.7 reduce-scatter.1
where the time goes:
time: 222 us; the launch traced here: 220 us
  other arithmetic  49.3 us (22%)
  waiting for transfers between devices  46.6 us (21%)
  blocking collectives  38.4 us (17%)
  matrix products  37.1 us (17%)
  starting transfers between devices  17 us (8%)
  local copies, waits for them, and re-layouts  16.1 us (7%)
  between operations  15.2 us (7%)
    another operation x2, other arithmetic, block_terms(): jax.scipy.linalg.solve_triangular(system, rhs_cols, lower=True, unit_diag...  39.3 us
    all_gather x4, blocking collectives, entering(): pieces = jax.tree.map(lambda part: lax.all_gather(part, axis), subtotal)  38.4 us
    all_to_all x1, waiting for transfers between devices, shards(): lax.all_to_all(produced.astype(jnp.bfloat16), EP, split_axis=0, concat_ax...  19.2 us
    reduce_scatter x1, waiting for transfers between devices, shards(): lax.psum_scatter(jnp.dot(attn_rows, output_weight, preferred_element_type...  19.2 us
    all_to_all x2, starting transfers between devices, exchange_in_pieces(): lax.all_to_all(section, axis, split_axis=0, concat_axis=0, tiled=True)  12.9 us
    dot_general x1, matrix products, shards(): jnp.einsum('secf,efd->secd', hidden, down_piece, preferred_element_type=j...  10 us
    all_to_all x2, waiting for transfers between devices, exchange_in_pieces(): lax.all_to_all(section, axis, split_axis=0, concat_axis=0, tiled=True)  8.1 us
    dot_general x8, matrix products, carry_step(): jnp.einsum('rpq,rpd->rqd', decayed_keys, value_updates)  6.33 us
  transfers between devices with their start and end apart: 5, of which 3 were waited for; matrix products, arithmetic and copies ran while one was open for 46% of the time, Pallas kernels for 0%

commit v1 on v0

v1 whole, which is shorter than its diff:
```python
import jax
import jax.numpy as jnp
from jax import lax
from jax.experimental import pallas as pl
from jax.experimental.pallas import tpu as pltpu
from jax.sharding import PartitionSpec as P

f32 = jnp.float32
bf16 = jnp.bfloat16
MESH = pl.DeviceIdType.MESH
EPS = 1e-06
SEG = 512
DH = 128
W = 2048
CAP = 32
EXPERTS = 16
EP = 16
NZ = 8
SH = 64
TOK = 128
SLOTS = EXPERTS * CAP


def dg(a, b, ca=1, cb=0):
    return lax.dot_general(a, b, (((ca,), (cb,)), ((), ())), preferred_element_type=f32)


def bdot(a, b, ca=1, cb=0):
    return dg(a.astype(bf16), b.astype(bf16), ca, cb)


def halves(a):
    hi = a.astype(bf16)
    return hi, (a - hi.astype(f32)).astype(bf16)


def dot3(a, b, ca=1, cb=0):
    ah, al = halves(a)
    bh, bl = halves(b)
    return dg(ah, bh, ca, cb) + dg(ah, bl, ca, cb) + dg(al, bh, ca, cb)


def iota(shape, dim):
    return lax.broadcasted_iota(jnp.int32, shape, dim)


def softplus(a):
    return jnp.maximum(a, 0.0) + jnp.log(1.0 + jnp.exp(-jnp.abs(a)))


def sigmoid(a):
    return 1.0 / (1.0 + jnp.exp(-a))


def kernel(
    q_ref, k_ref, v_ref, lg_ref, pre_ref, hdl_ref, ex_ref, wo_ref,
    tok_ref, sc_ref, ch_ref, grw_ref, eld_ref, wg_ref, wu_ref, wd_ref,
    o1_ref, o2_ref,
    gu, dw, obuf, xbuf, ybuf, rbuf, acc,
    a_s, s_s, x_s, ol_s, p_s, m_s, st_own, st_all, att_s,
    mine, theirs, pbuf, rrp, rrm, rsp, rsm,
    sp, rp, sm, rm, ps, pr, dsend, drecv, bsend, brecv, ssend, srecv, xs, qs_p, qr_p, qs_m, qr_m,
):
    ep = lax.axis_index("ep")
    tp = lax.axis_index("tp")
    z, c = tp // 2, tp % 2
    y, x = ep // 4, ep % 4
    up = ((z + 1) % NZ) * 2 + c
    down = ((z + NZ - 1) % NZ) * 2 + c
    mate = tp + 1 - 2 * c

    def peer(i):
        return ((y + i // 4) % 4) * 4 + (x + i % 4) % 4

    barrier = pltpu.get_barrier_semaphore()
    for i in range(1, EP):
        pl.semaphore_signal(barrier, inc=1, device_id={"ep": peer(i)}, device_id_type=MESH)
    for t in (up, down, mate):
        pl.semaphore_signal(barrier, inc=1, device_id={"tp": t}, device_id_type=MESH)
    pl.semaphore_wait(barrier, EP - 1 + 3)

    def remote(src, dst, send, recv, **where):
        return pltpu.make_async_remote_copy(
            src_ref=src, dst_ref=dst, send_sem=send, recv_sem=recv, device_id=where, device_id_type=MESH
        )

    def place(zs, core, piece, rows):
        whole = dw.at[zs, core] if piece == 2 else gu.at[zs, piece, core]
        return whole if rows is None else whole.at[pl.ds(rows, SH // 2)]

    own = (wg_ref.at[0], wu_ref.at[0], wd_ref.at[0])

    def ring(s, piece, forward):
        slot = (z + NZ - s) % NZ if forward else (z + s) % NZ
        rows = None if s < 3 else (0 if forward else SH // 2)
        src = own[piece] if s == 0 else place(slot, c, piece, rows)
        dst = place(slot, c, piece, rows)
        if forward:
            return remote(src, dst, sp.at[s, piece], rp.at[s, piece], tp=up)
        return remote(src, dst, sm.at[s, piece], rm.at[s, piece], tp=down)

    def across(n, piece):
        if n == 0:
            slot, rows = z, None
        elif n <= 3:
            slot, rows = (z + NZ - n) % NZ, None
        elif n <= 6:
            slot, rows = (z + n - 3) % NZ, None
        else:
            slot, rows = (z + 4) % NZ, (0 if n == 7 else SH // 2)
        src = own[piece] if n == 0 else place(slot, c, piece, rows)
        return remote(src, place(slot, c, piece, rows), ps.at[n, piece], pr.at[n, piece], tp=mate)

    for piece in range(3):
        ring(0, piece, True).start()
        ring(0, piece, False).start()
    for piece in range(3):
        across(0, piece).start()

    def pump(s, piece):
        ring(s - 1, piece, True).wait_recv()
        if s < 4:
            ring(s, piece, True).start()
        across(s if s < 4 else 7, piece).start()
        ring(s - 1, piece, False).wait_recv()
        if s < 4:
            ring(s, piece, False).start()
        across(3 + s if s < 4 else 8, piece).start()

    gu[z, 0, c] = wg_ref[0]
    gu[z, 1, c] = wu_ref[0]
    dw[z, c] = wd_ref[0]

    wide = tok_ref[...].astype(f32)
    normed = (
        wide * lax.rsqrt(jnp.sum(wide * wide, axis=1, keepdims=True) * (1.0 / W) + EPS) * sc_ref[...]
    ).astype(bf16)
    first, second = ch_ref[:, 0:1], ch_ref[:, 1:2]
    lane16 = iota((TOK, EXPERTS), 1)
    is_first, is_second = lane16 == first, lane16 == second
    member = jnp.where(is_first | is_second, 1.0, 0.0)
    before = jnp.where(iota((TOK, TOK), 1) < iota((TOK, TOK), 0), 1.0, 0.0)
    spot = bdot(before, member) + (lane16 * CAP).astype(f32)
    slot1 = jnp.sum(jnp.where(is_first, spot, 0.0), axis=1, keepdims=True).astype(jnp.int32)
    slot2 = jnp.sum(jnp.where(is_second, spot, 0.0), axis=1, keepdims=True).astype(jnp.int32)
    lanes = iota((TOK, SLOTS), 1)
    pick1 = jnp.where(lanes == slot1, 1.0, 0.0).astype(bf16)
    pick2 = jnp.where(lanes == slot2, 1.0, 0.0).astype(bf16)
    obuf[...] = dg(pick1 + pick2, normed, 0, 0).astype(bf16)

    def dispatch(i):
        return remote(
            obuf.at[pl.ds(peer(i) * CAP, CAP)], xbuf.at[pl.ds(ep * CAP, CAP)], dsend.at[i], drecv.at[i], ep=peer(i)
        )

    def bring_back(i):
        return remote(
            ybuf.at[pl.ds(peer(i) * CAP, CAP)], rbuf.at[pl.ds(ep * CAP, CAP)], bsend.at[i], brecv.at[i], ep=peer(i)
        )

    for i in range(1, EP):
        dispatch(i).start()
    home = pl.ds(pl.multiple_of(ep * CAP, CAP), CAP)
    xbuf[home, :] = obuf[home, :]

    kb, qb = k_ref[...], q_ref[...]
    ld = -jnp.exp(hdl_ref[...]) * softplus(pre_ref[...].astype(f32)) + ex_ref[...]
    beta = sigmoid(lg_ref[...].astype(f32))
    kf = kb.astype(f32)
    k2h, k2l = halves(kf * kf)
    ones = jnp.ones((8, DH), bf16)
    rk_row = lax.rsqrt((dg(ones, k2h, 1, 1) + dg(ones, k2l, 1, 1))[0:1] + EPS)
    upper = jnp.where(iota((SEG, SEG), 0) <= iota((SEG, SEG), 1), 1.0, 0.0).astype(bf16)
    ld8 = jnp.broadcast_to(ld, (8, SEG))
    l1, rest = halves(ld8)
    l2 = (ld8 - l1.astype(f32) - rest.astype(f32)).astype(bf16)
    c_row = (dg(l1, upper) + dg(rest, upper) + dg(l2, upper))[0:1]
    last = c_row[:, SEG - 1 : SEG]
    rhs, kds, qds = [], [], []
    for n in range(SEG // DH):
        rows = slice(n * DH, (n + 1) * DH)
        ii = iota((DH, SEG), 0) + n * DH
        jj = iota((DH, SEG), 1)
        c_col = jnp.sum(jnp.where(jj <= ii, ld, 0.0), axis=1, keepdims=True)
        b_col = jnp.sum(jnp.where(jj == ii, beta, 0.0), axis=1, keepdims=True)
        kt = kf[rows]
        qt = qb[rows].astype(f32)
        rk_col = lax.rsqrt(jnp.sum(kt * kt, axis=1, keepdims=True) + EPS)
        rq_col = lax.rsqrt(jnp.sum(qt * qt, axis=1, keepdims=True) + EPS) * DH**-0.5
        decay = jnp.where(ii >= jj, jnp.exp(jnp.minimum(c_col - c_row, 0.0)), 0.0) * rk_row
        a_s[rows, :] = jnp.where(ii > jj, dg(kb[rows], kb, 1, 1) * decay * (b_col * rk_col), 0.0)
        s_s[rows, :] = dg(qb[rows], kb, 1, 1) * decay * rq_col
        kn = kt * rk_col
        ec = jnp.exp(c_col)
        rhs.append(jnp.concatenate([b_col * v_ref[rows, :].astype(f32), (b_col * ec) * kn], axis=1))
        p_s[rows, :] = qt * (rq_col * ec)
        ol_s[rows, :] = kn * jnp.exp(last - c_col)
    for n in range(SEG // DH):
        x_s[n * DH : (n + 1) * DH, :] = rhs[n]

    pump(1, 0)

    half = SEG // 2
    i2, j2 = iota((half, half), 0), iota((half, half), 1)

    def same(shift):
        return (i2 >> shift) == (j2 >> shift)

    big = [a_s[0:half, 0:half], a_s[half:, half:]]
    power = [jnp.where(same(4), -b, 0.0) for b in big]
    inv = [jnp.where(i2 == j2, 1.0, 0.0) + p for p in power]
    for _ in range(3):
        power = [dot3(p, p) for p in power]
        inv = [t + dot3(t, p) for t, p in zip(inv, power)]
    pump(1, 1)
    for shift in (4, 5, 6, 7):
        off = [jnp.where(same(shift + 1) & ~same(shift), b, 0.0) for b in big]
        mid = [dot3(t, o) for t, o in zip(inv, off)]
        inv = [t - dot3(m, t) for t, m in zip(inv, mid)]
    x1 = dot3(inv[0], x_s[0:half, :])
    x2 = dot3(inv[1], x_s[half:, :] - dot3(a_s[half:, 0:half], x1))
    x_s[0:half, :] = x1
    x_s[half:, :] = x2
    e = dot3(ol_s[...], x_s[...], 0, 0)
    diag = iota((DH, DH), 0) == iota((DH, DH), 1)
    st_own[:, 0:DH] = (jnp.where(diag, jnp.exp(last), 0.0) - e[:, DH:]).astype(bf16)
    st_own[:, DH:] = e[:, :DH].astype(bf16)

    def state(j):
        return remote(st_own, st_all.at[ep], ssend.at[j], srecv.at[ep], ep=j)

    for j in range(1, EP):

        @pl.when(ep < j)
        def _(j=j):
            state(j).start()

    sx = dot3(s_s[...], x_s[...])
    ol_s[...] = sx[:, :DH]
    p_s[...] = p_s[...] - sx[:, DH:]

    pump(1, 2)

    def experts(slots, start, size, begin):
        xt = xbuf[pl.ds(start, size), :]
        total = None
        for zs in slots:
            both = dg(xt, gu[zs].reshape(4 * SH, W), 1, 1)
            g, u = both[:, : 2 * SH], both[:, 2 * SH :]
            h = (g * sigmoid(g) * u).astype(bf16)
            part = dg(h, dw[zs].reshape(2 * SH, W))
            total = part if total is None else total + part
        return total if begin else acc[pl.ds(start, size), :] + total

    MT = 128

    def group(s):
        for n in ((0,) if s == 0 else (s, 3 + s)):
            for piece in range(3):
                across(n, piece).wait_recv()
        slots = (z,) if s == 0 else ((z + NZ - s) % NZ, (z + s) % NZ)

        def body(m, carry):
            start = pl.multiple_of(m * MT, MT)
            acc[pl.ds(start, MT), :] = experts(slots, start, MT, s == 0)
            return carry

        lax.fori_loop(0, SEG // MT, body, 0)

    for i in range(1, EP):
        dispatch(i).wait_recv()
    group(0)
    pump(2, 0)

    m_s[...] = jnp.zeros((DH, DH), f32)
    for j in range(EP - 1):

        @pl.when(j < ep)
        def _(j=j):
            remote(st_own, st_all.at[j], ssend.at[0], srecv.at[j], ep=0).wait_recv()
            m_s[...] = bdot(st_all[j, :, 0:DH], m_s[...]) + st_all[j, :, DH:].astype(f32)

    att = (ol_s[...] + bdot(p_s[...], m_s[...])).astype(bf16)
    att_s[...] = att.reshape(NZ, 2, CAP, DH)
    pump(2, 1)
    theirs[...] = dg(att_s[:, 1 - c].reshape(SEG // 2, DH), wo_ref[...]).astype(bf16).reshape(NZ, CAP, W)
    swap = remote(theirs, pbuf, xs.at[0], xs.at[1], tp=mate)
    swap.start()
    mine[...] = dg(att_s[:, c].reshape(SEG // 2, DH), wo_ref[...]).reshape(NZ, CAP, W)
    pump(2, 2)
    group(1)
    pump(3, 0)
    swap.wait_recv()

    def grow(zs):
        return mine[zs] + pbuf[zs].astype(f32)

    def sums(s, forward):
        if forward:
            return remote(rsp.at[s], rrp.at[s], qs_p.at[s], qr_p.at[s], tp=up)
        return remote(rsm.at[s], rrm.at[s], qs_m.at[s], qr_m.at[s], tp=down)

    rsp[0] = grow((z + 4) % NZ).astype(bf16)
    rsm[0] = grow((z + NZ - 3) % NZ).astype(bf16)
    pump(3, 1)
    group(2)
    pump(3, 2)
    sums(0, True).start()
    sums(0, False).start()
    group(3)
    for piece in range(3):
        pump(4, piece)

    for n in (7, 8):
        for piece in range(3):
            across(n, piece).wait_recv()
    for i in range(4):
        yy = (y + i) % 4
        start = pl.multiple_of(yy * (4 * CAP), 4 * CAP)
        ybuf[pl.ds(start, 4 * CAP), :] = experts(((z + 4) % NZ,), start, 4 * CAP, False).astype(bf16)
        for n in range(4):
            if i + n:
                bring_back(4 * i + n).start()
    rbuf[home, :] = ybuf[home, :]

    for s in range(1, 4):
        sums(s - 1, True).wait_recv()
        rsp[s] = (rrp[s - 1].astype(f32) + grow((z + 4 - s) % NZ)).astype(bf16)
        sums(s, True).start()
        if s < 3:
            sums(s - 1, False).wait_recv()
            rsm[s] = (rrm[s - 1].astype(f32) + grow((z + NZ - 3 + s) % NZ)).astype(bf16)
            sums(s, False).start()
    sums(2, False).wait_recv()
    sums(3, True).wait_recv()
    o1_ref[...] = (grow(z) + rrp[3].astype(f32) + rrm[2].astype(f32)).astype(bf16)

    diag = iota((TOK, TOK), 0) == iota((TOK, TOK), 1)
    lead = sigmoid(eld_ref[...])
    w1 = jnp.sum(jnp.where(diag, grw_ref[...] * lead, 0.0), axis=1, keepdims=True)
    w2 = jnp.sum(jnp.where(diag, grw_ref[...] * (1.0 - lead), 0.0), axis=1, keepdims=True)
    for i in range(1, EP):
        bring_back(i).wait_recv()
    o2_ref[...] = (w1 * dg(pick1, rbuf[...]) + w2 * dg(pick2, rbuf[...])).astype(bf16)

    for s in range(4):
        for piece in range(3):
            ring(s, piece, True).wait_send()
            ring(s, piece, False).wait_send()
        sums(s, True).wait_send()
        if s < 3:
            sums(s, False).wait_send()
    for n in range(9):
        for piece in range(3):
            across(n, piece).wait_send()
    for i in range(1, EP):
        dispatch(i).wait_send()
        bring_back(i).wait_send()
    swap.wait_send()
    for j in range(1, EP):

        @pl.when(ep < j)
        def _(j=j):
            state(j).wait_send()


def shards(q, k, v, lg, pre, hdl, ex, wo, tok, sc, ch, grw, eld, wg, wu, wd):
    V = pltpu.VMEM
    dma = pltpu.SemaphoreType.DMA
    scratch = [
        V((NZ, 2, 2, SH, W), bf16), V((NZ, 2, SH, W), bf16),
        V((SLOTS, W), bf16), V((SLOTS, W), bf16), V((SLOTS, W), bf16), V((SLOTS, W), bf16), V((SLOTS, W), f32),
        V((SEG, SEG), f32), V((SEG, SEG), f32), V((SEG, 2 * DH), f32), V((SEG, DH), f32), V((SEG, DH), f32),
        V((DH, DH), f32), V((DH, 2 * DH), bf16), V((EP, DH, 2 * DH), bf16), V((NZ, 2, CAP, DH), bf16),
        V((NZ, CAP, W), f32), V((NZ, CAP, W), bf16), V((NZ, CAP, W), bf16),
        V((4, CAP, W), bf16), V((3, CAP, W), bf16), V((4, CAP, W), bf16), V((3, CAP, W), bf16),
        dma((4, 3)), dma((4, 3)), dma((4, 3)), dma((4, 3)), dma((9, 3)), dma((9, 3)),
        dma((EP,)), dma((EP,)), dma((EP,)), dma((EP,)), dma((EP,)), dma((EP,)), dma((2,)),
        dma((4,)), dma((4,)), dma((3,)), dma((3,)),
    ]
    return pl.pallas_call(
        kernel,
        name="mixer_and_experts",
        out_shape=(jax.ShapeDtypeStruct((CAP, W), bf16), jax.ShapeDtypeStruct((TOK, W), bf16)),
        in_specs=[pl.BlockSpec(memory_space=pltpu.VMEM)] * 16,
        out_specs=(pl.BlockSpec(memory_space=pltpu.VMEM),) * 2,
        scratch_shapes=scratch,
        compiler_params=pltpu.CompilerParams(
            collective_id=0, has_side_effects=True, vmem_limit_bytes=60 * 1024 * 1024
        ),
    )(
        q, k, v, lg, pre, hdl.reshape(1, 1), ex, wo,
        tok, sc.reshape(1, W), ch, grw.reshape(1, TOK), eld.reshape(1, TOK), wg, wu, wd,
    )


def solution(mesh):
    both = ("ep", "tp")
    placed = (
        P("ep", "tp"), P("ep", "tp"), P("ep", "tp"),
        P("tp", "ep"), P("tp", "ep"), P("tp"), P("tp", "ep"), P("tp", None),
        P(both, None), P(), P(both, None), P(both), P(both),
        P("ep", "tp", None), P("ep", "tp", None), P("ep", "tp", None),
    )
    return jax.shard_map(
        shards, mesh=mesh, in_specs=placed, out_specs=(P(both, None), P(both, None)), check_vma=False
    )
```

time: 222 us -> 129 us (0.58)
  the two profiles are of different devices: /device:TPU:1 before, /device:TPU:17 now
where the time goes in v1:
time: 129 us
  Pallas kernels  123 us (95%)
  local copies, waits for them, and re-layouts  4.86 us (4%)
  between operations  1.29 us (1%)
    pallas_call x1, Pallas kernels, shards(): pl.pallas_call(kernel, name='mixer_and_experts', out_shape=(jax.ShapeDtyp...  123 us
    unnamed x5, local copies, waits for them, and re-layouts  4.86 us

profile of v1, /device:TPU:17, one launch (start us, length us, event | category | flops | bytes accessed | tf_op | source)
XLA Modules:
  0.0 128.7 jit_solution(11333193536418422773)
XLA Ops:
  1.3 0.0 copy-start
  1.3 0.7 copy-done
  2.0 0.7 copy.18.ch_ref
  2.7 122.6 %mixer_and_experts.1 = (bf16[32,2048]{1,0:T(8,128)(2,1)}, bf16[128,2048]{1,0:T(8,128)(2,1)}) custom-call(bf16[512,128]{1,0:T(8,128)(2,1)} %q_ref.1, bf16[512,128]{1,0:T(8,128)(2,1)} %k_ref.1, bf16[512,128]{1,0:T(8,128)(2,1)} %v_ref.1, bf16[1,512]{1,0:T(2,128)(2,1)} %lg_ref.1, bf16[1,512]{1,0:T(2,128)(2,1)} %pre_ref.1, f32[1,1]{1,0:T(1,128)} %bitcast.4.hdl_ref, ...), custom_call_target="tpu_custom_call" | custom-call | tf_op jit(solution)/shard_map/mixer_and_experts/pallas_call | solution.py:381
  125.3 1.6 %copy.22 = bf16[32,2048]{1,0:T(8,128)(2,1)} copy(bf16[32,2048]{1,0:T(8,128)(2,1)} %get-tuple-element.4) | data formatting | bytes 262144
  126.9 1.9 %copy.23 = bf16[128,2048]{1,0:T(8,128)(2,1)} copy(bf16[128,2048]{1,0:T(8,128)(2,1)} %get-tuple-element.5) | data formatting | bytes 1048576
Async XLA Ops:
  1.3 0.7 copy-start

commit v2 on v1

--- a/solution.py
+++ b/solution.py
@@ -19,6 +19,13 @@
 SH = 64
 TOK = 128
 SLOTS = EXPERTS * CAP
+RELAY = {10: 15, 8: 4, 9: 13, 11: 7, 6: 7, 14: 13, 2: 1}
+ORDER = list(RELAY)
+DIRECT = [i for i in range(1, 16) if i not in RELAY]
+
+
+def minus(i, j):
+    return ((i // 4 - j // 4) % 4) * 4 + (i % 4 - j % 4) % 4
 
 
 def dg(a, b, ca=1, cb=0):
@@ -53,13 +60,15 @@
 
 
 def kernel(
-    q_ref, k_ref, v_ref, lg_ref, pre_ref, hdl_ref, ex_ref, wo_ref,
-    tok_ref, sc_ref, ch_ref, grw_ref, eld_ref, wg_ref, wu_ref, wd_ref,
+    q_hbm, k_hbm, v_hbm, lg_ref, pre_ref, hdl_ref, ex_ref, wo_hbm,
+    tok_hbm, sc_ref, ch_ref, grw_ref, eld_ref, wg_hbm, wu_hbm, wd_hbm,
     o1_ref, o2_ref,
-    gu, dw, obuf, xbuf, ybuf, rbuf, acc,
+    q_ref, k_ref, v_ref, wo_ref, tok_ref,
+    gu, dw, obuf, xbuf, ybuf, rbuf, acc, dhop, bhop, h_s,
     a_s, s_s, x_s, ol_s, p_s, m_s, st_own, st_all, att_s,
     mine, theirs, pbuf, rrp, rrm, rsp, rsm,
-    sp, rp, sm, rm, ps, pr, dsend, drecv, bsend, brecv, ssend, srecv, xs, qs_p, qr_p, qs_m, qr_m,
+    sp, rp, sm, rm, ps, pr, dsend, drecv, dhs, dhr, bsend, brecv, bhs, bhr,
+    ssend, srecv, xs, qs_p, qr_p, qs_m, qr_m, ins,
 ):
     ep = lax.axis_index("ep")
     tp = lax.axis_index("tp")
@@ -72,6 +81,16 @@
     def peer(i):
         return ((y + i // 4) % 4) * 4 + (x + i % 4) % 4
 
+    def loaded(n):
+        pairs = (
+            (wg_hbm.at[0], gu.at[z, 0, c]), (wu_hbm.at[0], gu.at[z, 1, c]), (wd_hbm.at[0], dw.at[z, c]),
+            (tok_hbm, tok_ref), (k_hbm, k_ref), (q_hbm, q_ref), (v_hbm, v_ref), (wo_hbm, wo_ref),
+        )
+        return pltpu.make_async_copy(*pairs[n], ins.at[n])
+
+    for n in range(8):
+        loaded(n).start()
+
     barrier = pltpu.get_barrier_semaphore()
     for i in range(1, EP):
         pl.semaphore_signal(barrier, inc=1, device_id={"ep": peer(i)}, device_id_type=MESH)
@@ -88,16 +107,13 @@
         whole = dw.at[zs, core] if piece == 2 else gu.at[zs, piece, core]
         return whole if rows is None else whole.at[pl.ds(rows, SH // 2)]
 
-    own = (wg_ref.at[0], wu_ref.at[0], wd_ref.at[0])
-
     def ring(s, piece, forward):
         slot = (z + NZ - s) % NZ if forward else (z + s) % NZ
         rows = None if s < 3 else (0 if forward else SH // 2)
-        src = own[piece] if s == 0 else place(slot, c, piece, rows)
-        dst = place(slot, c, piece, rows)
+        here = place(slot, c, piece, rows)
         if forward:
-            return remote(src, dst, sp.at[s, piece], rp.at[s, piece], tp=up)
-        return remote(src, dst, sm.at[s, piece], rm.at[s, piece], tp=down)
+            return remote(here, here, sp.at[s, piece], rp.at[s, piece], tp=up)
+        return remote(here, here, sm.at[s, piece], rm.at[s, piece], tp=down)
 
     def across(n, piece):
         if n == 0:
@@ -108,9 +124,11 @@
             slot, rows = (z + n - 3) % NZ, None
         else:
             slot, rows = (z + 4) % NZ, (0 if n == 7 else SH // 2)
-        src = own[piece] if n == 0 else place(slot, c, piece, rows)
-        return remote(src, place(slot, c, piece, rows), ps.at[n, piece], pr.at[n, piece], tp=mate)
-
+        here = place(slot, c, piece, rows)
+        return remote(here, here, ps.at[n, piece], pr.at[n, piece], tp=mate)
+
+    for piece in range(3):
+        loaded(piece).wait()
     for piece in range(3):
         ring(0, piece, True).start()
         ring(0, piece, False).start()
@@ -127,15 +145,14 @@
             ring(s, piece, False).start()
         across(3 + s if s < 4 else 8, piece).start()
 
-    gu[z, 0, c] = wg_ref[0]
-    gu[z, 1, c] = wu_ref[0]
-    dw[z, c] = wd_ref[0]
-
+    loaded(3).wait()
     wide = tok_ref[...].astype(f32)
     normed = (
         wide * lax.rsqrt(jnp.sum(wide * wide, axis=1, keepdims=True) * (1.0 / W) + EPS) * sc_ref[...]
     ).astype(bf16)
-    first, second = ch_ref[:, 0:1], ch_ref[:, 1:2]
+    eye = iota((TOK, TOK), 0) == iota((TOK, TOK), 1)
+    first = jnp.sum(jnp.where(eye, ch_ref[0:1, :], 0), axis=1, keepdims=True)
+    second = jnp.sum(jnp.where(eye, ch_ref[1:2, :], 0), axis=1, keepdims=True)
     lane16 = iota((TOK, EXPERTS), 1)
     is_first, is_second = lane16 == first, lane16 == second
     member = jnp.where(is_first | is_second, 1.0, 0.0)
@@ -148,23 +165,46 @@
     pick2 = jnp.where(lanes == slot2, 1.0, 0.0).astype(bf16)
     obuf[...] = dg(pick1 + pick2, normed, 0, 0).astype(bf16)
 
-    def dispatch(i):
-        return remote(
-            obuf.at[pl.ds(peer(i) * CAP, CAP)], xbuf.at[pl.ds(ep * CAP, CAP)], dsend.at[i], drecv.at[i], ep=peer(i)
-        )
-
-    def bring_back(i):
-        return remote(
-            ybuf.at[pl.ds(peer(i) * CAP, CAP)], rbuf.at[pl.ds(ep * CAP, CAP)], bsend.at[i], brecv.at[i], ep=peer(i)
-        )
-
-    for i in range(1, EP):
-        dispatch(i).start()
+    def route(src, dst, hop, send, recv, hsend, hrecv):
+        def first_leg(i):
+            block = src.at[pl.ds(peer(i) * CAP, CAP)]
+            if i in RELAY:
+                n = ORDER.index(i)
+                return remote(block, hop.at[n], send.at[i], hrecv.at[n], ep=peer(RELAY[i]))
+            return remote(block, dst.at[pl.ds(ep * CAP, CAP)], send.at[i], recv.at[i], ep=peer(i))
+
+        def second_leg(i):
+            n = ORDER.index(i)
+            origin = peer(minus(0, RELAY[i]))
+            there = dst.at[pl.ds(origin * CAP, CAP)]
+            return remote(hop.at[n], there, hsend.at[n], recv.at[i], ep=peer(minus(i, RELAY[i])))
+
+        def last(i):
+            return remote(src.at[pl.ds(0, CAP)], dst.at[pl.ds(0, CAP)], send.at[i], recv.at[i], ep=peer(i))
+
+        def forward(i):
+            first_leg(i).wait_recv()
+            second_leg(i).start()
+
+        def drain():
+            for i in range(1, EP):
+                first_leg(i).wait_send()
+            for i in ORDER:
+                second_leg(i).wait_send()
+
+        return first_leg, forward, last, drain
+
+    d_first, d_forward, d_last, d_drain = route(obuf, xbuf, dhop, dsend, drecv, dhs, dhr)
+    b_first, b_forward, b_last, b_drain = route(ybuf, rbuf, bhop, bsend, brecv, bhs, bhr)
+    for i in ORDER + DIRECT:
+        d_first(i).start()
     home = pl.ds(pl.multiple_of(ep * CAP, CAP), CAP)
     xbuf[home, :] = obuf[home, :]
 
+    for n in (4, 5, 6):
+        loaded(n).wait()
     kb, qb = k_ref[...], q_ref[...]
-    ld = -jnp.exp(hdl_ref[...]) * softplus(pre_ref[...].astype(f32)) + ex_ref[...]
+    ld = -jnp.exp(jnp.full((1, 1), hdl_ref[0], f32)) * softplus(pre_ref[...].astype(f32)) + ex_ref[...]
     beta = sigmoid(lg_ref[...].astype(f32))
     kf = kb.astype(f32)
     k2h, k2l = halves(kf * kf)
@@ -198,8 +238,6 @@
     for n in range(SEG // DH):
         x_s[n * DH : (n + 1) * DH, :] = rhs[n]
 
-    pump(1, 0)
-
     half = SEG // 2
     i2, j2 = iota((half, half), 0), iota((half, half), 1)
 
@@ -212,7 +250,6 @@
     for _ in range(3):
         power = [dot3(p, p) for p in power]
         inv = [t + dot3(t, p) for t, p in zip(inv, power)]
-    pump(1, 1)
     for shift in (4, 5, 6, 7):
         off = [jnp.where(same(shift + 1) & ~same(shift), b, 0.0) for b in big]
         mid = [dot3(t, o) for t, o in zip(inv, off)]
@@ -235,11 +272,17 @@
         def _(j=j):
             state(j).start()
 
+    pump(1, 0)
     sx = dot3(s_s[...], x_s[...])
     ol_s[...] = sx[:, :DH]
     p_s[...] = p_s[...] - sx[:, DH:]
-
+    for i in ORDER[:4]:
+        d_forward(i)
+    pump(1, 1)
+    for i in ORDER[4:]:
+        d_forward(i)
     pump(1, 2)
+    pump(2, 0)
 
     def experts(slots, start, size, begin):
         xt = xbuf[pl.ds(start, size), :]
@@ -252,7 +295,7 @@
             total = part if total is None else total + part
         return total if begin else acc[pl.ds(start, size), :] + total
 
-    MT = 128
+    MT = 256
 
     def group(s):
         for n in ((0,) if s == 0 else (s, 3 + s)):
@@ -268,9 +311,10 @@
         lax.fori_loop(0, SEG // MT, body, 0)
 
     for i in range(1, EP):
-        dispatch(i).wait_recv()
+        d_last(i).wait_recv()
     group(0)
-    pump(2, 0)
+    pump(2, 1)
+    group(1)
 
     m_s[...] = jnp.zeros((DH, DH), f32)
     for j in range(EP - 1):
@@ -282,13 +326,12 @@
 
     att = (ol_s[...] + bdot(p_s[...], m_s[...])).astype(bf16)
     att_s[...] = att.reshape(NZ, 2, CAP, DH)
-    pump(2, 1)
+    loaded(7).wait()
     theirs[...] = dg(att_s[:, 1 - c].reshape(SEG // 2, DH), wo_ref[...]).astype(bf16).reshape(NZ, CAP, W)
     swap = remote(theirs, pbuf, xs.at[0], xs.at[1], tp=mate)
     swap.start()
     mine[...] = dg(att_s[:, c].reshape(SEG // 2, DH), wo_ref[...]).reshape(NZ, CAP, W)
     pump(2, 2)
-    group(1)
     pump(3, 0)
     swap.wait_recv()
 
@@ -308,21 +351,29 @@
     sums(0, True).start()
     sums(0, False).start()
     group(3)
-    for piece in range(3):
+    far = (z + 4) % NZ
+    for piece in range(2):
         pump(4, piece)
-
     for n in (7, 8):
-        for piece in range(3):
+        for piece in range(2):
             across(n, piece).wait_recv()
-    for i in range(4):
-        yy = (y + i) % 4
-        start = pl.multiple_of(yy * (4 * CAP), 4 * CAP)
-        ybuf[pl.ds(start, 4 * CAP), :] = experts(((z + 4) % NZ,), start, 4 * CAP, False).astype(bf16)
-        for n in range(4):
+    both = dg(xbuf[...], gu[far].reshape(4 * SH, W), 1, 1)
+    g, u = both[:, : 2 * SH], both[:, 2 * SH :]
+    h_s[...] = (g * sigmoid(g) * u).astype(bf16)
+    pump(4, 2)
+    for n in (7, 8):
+        across(n, 2).wait_recv()
+    for i in (2, 1, 3, 0):
+        start = pl.multiple_of(((y + i) % 4) * (4 * CAP), 4 * CAP)
+        part = pl.ds(start, 4 * CAP)
+        ybuf[part, :] = (acc[part, :] + dg(h_s[part, :], dw[far].reshape(2 * SH, W))).astype(bf16)
+        for n in (2, 0, 1, 3):
             if i + n:
-                bring_back(4 * i + n).start()
+                b_first(4 * i + n).start()
     rbuf[home, :] = ybuf[home, :]
 
+    for i in ORDER[:3]:
+        b_forward(i)
     for s in range(1, 4):
         sums(s - 1, True).wait_recv()
         rsp[s] = (rrp[s - 1].astype(f32) + grow((z + 4 - s) % NZ)).astype(bf16)
@@ -331,16 +382,17 @@
             sums(s - 1, False).wait_recv()
             rsm[s] = (rrm[s - 1].astype(f32) + grow((z + NZ - 3 + s) % NZ)).astype(bf16)
             sums(s, False).start()
+        for i in ORDER[1 + 2 * s : 3 + 2 * s]:
+            b_forward(i)
     sums(2, False).wait_recv()
     sums(3, True).wait_recv()
     o1_ref[...] = (grow(z) + rrp[3].astype(f32) + rrm[2].astype(f32)).astype(bf16)
 
-    diag = iota((TOK, TOK), 0) == iota((TOK, TOK), 1)
     lead = sigmoid(eld_ref[...])
-    w1 = jnp.sum(jnp.where(diag, grw_ref[...] * lead, 0.0), axis=1, keepdims=True)
-    w2 = jnp.sum(jnp.where(diag, grw_ref[...] * (1.0 - lead), 0.0), axis=1, keepdims=True)
+    w1 = jnp.sum(jnp.where(eye, grw_ref[...] * lead, 0.0), axis=1, keepdims=True)
+    w2 = jnp.sum(jnp.where(eye, grw_ref[...] * (1.0 - lead), 0.0), axis=1, keepdims=True)
     for i in range(1, EP):
-        bring_back(i).wait_recv()
+        b_last(i).wait_recv()
     o2_ref[...] = (w1 * dg(pick1, rbuf[...]) + w2 * dg(pick2, rbuf[...])).astype(bf16)
 
     for s in range(4):
@@ -353,9 +405,8 @@
     for n in range(9):
         for piece in range(3):
             across(n, piece).wait_send()
-    for i in range(1, EP):
-        dispatch(i).wait_send()
-        bring_back(i).wait_send()
+    d_drain()
+    b_drain()
     swap.wait_send()
     for j in range(1, EP):
 
@@ -368,30 +419,47 @@
     V = pltpu.VMEM
     dma = pltpu.SemaphoreType.DMA
     scratch = [
+        V((SEG, DH), bf16), V((SEG, DH), bf16), V((SEG, DH), bf16), V((DH, W), bf16), V((TOK, W), bf16),
         V((NZ, 2, 2, SH, W), bf16), V((NZ, 2, SH, W), bf16),
         V((SLOTS, W), bf16), V((SLOTS, W), bf16), V((SLOTS, W), bf16), V((SLOTS, W), bf16), V((SLOTS, W), f32),
+        V((7, CAP, W), bf16), V((7, CAP, W), bf16), V((SLOTS, 2 * SH), bf16),
         V((SEG, SEG), f32), V((SEG, SEG), f32), V((SEG, 2 * DH), f32), V((SEG, DH), f32), V((SEG, DH), f32),
         V((DH, DH), f32), V((DH, 2 * DH), bf16), V((EP, DH, 2 * DH), bf16), V((NZ, 2, CAP, DH), bf16),
         V((NZ, CAP, W), f32), V((NZ, CAP, W), bf16), V((NZ, CAP, W), bf16),
         V((4, CAP, W), bf16), V((3, CAP, W), bf16), V((4, CAP, W), bf16), V((3, CAP, W), bf16),
         dma((4, 3)), dma((4, 3)), dma((4, 3)), dma((4, 3)), dma((9, 3)), dma((9, 3)),
-        dma((EP,)), dma((EP,)), dma((EP,)), dma((EP,)), dma((EP,)), dma((EP,)), dma((2,)),
-        dma((4,)), dma((4,)), dma((3,)), dma((3,)),
+        dma((EP,)), dma((EP,)), dma((7,)), dma((7,)), dma((EP,)), dma((EP,)), dma((7,)), dma((7,)),
+        dma((EP,)), dma((EP,)), dma((2,)), dma((4,)), dma((4,)), dma((3,)), dma((3,)), dma((8,)),
     ]
-    return pl.pallas_call(
+    vm = pl.BlockSpec(memory_space=pltpu.VMEM)
+    hbm = pl.BlockSpec(memory_space=pl.ANY)
+    outs = pl.pallas_call(
         kernel,
         name="mixer_and_experts",
         out_shape=(jax.ShapeDtypeStruct((CAP, W), bf16), jax.ShapeDtypeStruct((TOK, W), bf16)),
-        in_specs=[pl.BlockSpec(memory_space=pltpu.VMEM)] * 16,
-        out_specs=(pl.BlockSpec(memory_space=pltpu.VMEM),) * 2,
+        in_specs=[hbm, hbm, hbm, vm, vm, pl.BlockSpec(memory_space=pltpu.SMEM), vm, hbm, hbm, vm, vm, vm, vm, hbm, hbm, hbm],
+        out_specs=(vm, vm),
         scratch_shapes=scratch,
         compiler_params=pltpu.CompilerParams(
             collective_id=0, has_side_effects=True, vmem_limit_bytes=60 * 1024 * 1024
         ),
     )(
-        q, k, v, lg, pre, hdl.reshape(1, 1), ex, wo,
-        tok, sc.reshape(1, W), ch, grw.reshape(1, TOK), eld.reshape(1, TOK), wg, wu, wd,
+        q, k, v, lg, pre, hdl, ex, wo,
+        tok, sc.reshape(1, W), ch.T, grw.reshape(1, TOK), eld.reshape(1, TOK), wg, wu, wd,
     )
+    return pl.pallas_call(
+        hand_over,
+        name="hand_over",
+        out_shape=(jax.ShapeDtypeStruct((CAP, W), bf16), jax.ShapeDtypeStruct((TOK, W), bf16)),
+        in_specs=[vm, vm],
+        out_specs=(vm, vm),
+        compiler_params=pltpu.CompilerParams(vmem_limit_bytes=60 * 1024 * 1024),
+    )(*outs)
+
+
+def hand_over(a_ref, b_ref, c_ref, d_ref):
+    c_ref[...] = a_ref[...]
+    d_ref[...] = b_ref[...]
 
 
 def solution(mesh):

time: 129 us -> 113 us (0.88)
  the two profiles are of different devices: /device:TPU:17 before, /device:TPU:1 now
where the time goes in v2:
time: 113 us
  Pallas kernels  112 us (99%)
  between operations  1.29 us (1%)
    pallas_call x1, Pallas kernels, shards(): pl.pallas_call(kernel, name='mixer_and_experts', out_shape=(jax.ShapeDtyp...  110 us

profile of v2, /device:TPU:1, one launch (start us, length us, event | category | flops | bytes accessed | tf_op | source)
XLA Modules:
  0.0 113.0 jit_solution(12383522433604221578)
XLA Ops:
  1.3 109.7 %mixer_and_experts.1 = (bf16[32,2048]{1,0:T(8,128)(2,1)}, bf16[128,2048]{1,0:T(8,128)(2,1)}) custom-call(bf16[512,128]{1,0:T(8,128)(2,1)} %q_hbm.1, bf16[512,128]{1,0:T(8,128)(2,1)} %k_hbm.1, bf16[512,128]{1,0:T(8,128)(2,1)} %v_hbm.1, bf16[1,512]{1,0:T(2,128)(2,1)} %lg_ref.1, bf16[1,512]{1,0:T(2,128)(2,1)} %pre_ref.1, f32[1]{0:T(128)S(6)} %copy.18.hdl_ref, ...), custom_call_target="tpu_custom_call" | custom-call | tf_op jit(solution)/shard_map/mixer_and_experts/pallas_call | solution.py:436
  111.0 2.0 %hand_over.1 = (bf16[32,2048]{1,0:T(8,128)(2,1)}, bf16[128,2048]{1,0:T(8,128)(2,1)}) custom-call(bf16[32,2048]{1,0:T(8,128)(2,1)} %get-tuple-element.4.a_ref, bf16[128,2048]{1,0:T(8,128)(2,1)} %get-tuple-element.5.b_ref), custom_call_target="tpu_custom_call" | custom-call | tf_op jit(solution)/shard_map/hand_over/pallas_call | solution.py:450

commit v3 on v2

--- a/solution.py
+++ b/solution.py
@@ -18,6 +18,9 @@
 NZ = 8
 SH = 64
 TOK = 128
+CHUNKS = 4
+COLS = W // CHUNKS
+PIECES = 2 + CHUNKS
 SLOTS = EXPERTS * CAP
 RELAY = {10: 15, 8: 4, 9: 13, 11: 7, 6: 7, 14: 13, 2: 1}
 ORDER = list(RELAY)
@@ -64,7 +67,7 @@
     tok_hbm, sc_ref, ch_ref, grw_ref, eld_ref, wg_hbm, wu_hbm, wd_hbm,
     o1_ref, o2_ref,
     q_ref, k_ref, v_ref, wo_ref, tok_ref,
-    gu, dw, obuf, xbuf, ybuf, rbuf, acc, dhop, bhop, h_s,
+    gu, dw, obuf, xbuf, ybuf, rbuf, dhop, bhop, h_s,
     a_s, s_s, x_s, ol_s, p_s, m_s, st_own, st_all, att_s,
     mine, theirs, pbuf, rrp, rrm, rsp, rsm,
     sp, rp, sm, rm, ps, pr, dsend, drecv, dhs, dhr, bsend, brecv, bhs, bhr,
@@ -83,12 +86,13 @@
 
     def loaded(n):
         pairs = (
-            (wg_hbm.at[0], gu.at[z, 0, c]), (wu_hbm.at[0], gu.at[z, 1, c]), (wd_hbm.at[0], dw.at[z, c]),
+            (wg_hbm.at[0], gu.at[z, 0, c]), (wu_hbm.at[0], gu.at[z, 1, c]),
             (tok_hbm, tok_ref), (k_hbm, k_ref), (q_hbm, q_ref), (v_hbm, v_ref), (wo_hbm, wo_ref),
+            *((wd_hbm.at[0, :, pl.ds(n * COLS, COLS)], dw.at[n, z, c]) for n in range(CHUNKS)),
         )
         return pltpu.make_async_copy(*pairs[n], ins.at[n])
 
-    for n in range(8):
+    for n in (0, 1, 7, 2, 3, 4, 5, 8, 9, 10, 6):
         loaded(n).start()
 
     barrier = pltpu.get_barrier_semaphore()
@@ -104,7 +108,7 @@
         )
 
     def place(zs, core, piece, rows):
-        whole = dw.at[zs, core] if piece == 2 else gu.at[zs, piece, core]
+        whole = gu.at[zs, piece, core] if piece < 2 else dw.at[piece - 2, zs, core]
         return whole if rows is None else whole.at[pl.ds(rows, SH // 2)]
 
     def ring(s, piece, forward):
@@ -127,25 +131,31 @@
         here = place(slot, c, piece, rows)
         return remote(here, here, ps.at[n, piece], pr.at[n, piece], tp=mate)
 
+    def step(piece, s):
+        if s == 0:
+            across(0, piece).start()
+            ring(0, piece, True).start()
+            ring(0, piece, False).start()
+            return
+        ring(s - 1, piece, True).wait_recv()
+        ring(s, piece, True).start()
+        across(s, piece).start()
+        ring(s - 1, piece, False).wait_recv()
+        ring(s, piece, False).start()
+        across(3 + s, piece).start()
+
+    def finish(piece):
+        ring(3, piece, True).wait_recv()
+        across(7, piece).start()
+        ring(3, piece, False).wait_recv()
+        across(8, piece).start()
+
+    for n in (0, 1, 7):
+        loaded(n).wait()
     for piece in range(3):
-        loaded(piece).wait()
-    for piece in range(3):
-        ring(0, piece, True).start()
-        ring(0, piece, False).start()
-    for piece in range(3):
-        across(0, piece).start()
-
-    def pump(s, piece):
-        ring(s - 1, piece, True).wait_recv()
-        if s < 4:
-            ring(s, piece, True).start()
-        across(s if s < 4 else 7, piece).start()
-        ring(s - 1, piece, False).wait_recv()
-        if s < 4:
-            ring(s, piece, False).start()
-        across(3 + s if s < 4 else 8, piece).start()
-
-    loaded(3).wait()
+        step(piece, 0)
+
+    loaded(2).wait()
     wide = tok_ref[...].astype(f32)
     normed = (
         wide * lax.rsqrt(jnp.sum(wide * wide, axis=1, keepdims=True) * (1.0 / W) + EPS) * sc_ref[...]
@@ -195,13 +205,16 @@
         return first_leg, forward, last, drain
 
     d_first, d_forward, d_last, d_drain = route(obuf, xbuf, dhop, dsend, drecv, dhs, dhr)
-    b_first, b_forward, b_last, b_drain = route(ybuf, rbuf, bhop, bsend, brecv, bhs, bhr)
+    back = [
+        route(ybuf.at[n], rbuf.at[n], bhop.at[n], bsend.at[n], brecv.at[n], bhs.at[n], bhr.at[n])
+        for n in range(CHUNKS)
+    ]
     for i in ORDER + DIRECT:
         d_first(i).start()
     home = pl.ds(pl.multiple_of(ep * CAP, CAP), CAP)
     xbuf[home, :] = obuf[home, :]
 
-    for n in (4, 5, 6):
+    for n in (3, 4, 5):
         loaded(n).wait()
     kb, qb = k_ref[...], q_ref[...]
     ld = -jnp.exp(jnp.full((1, 1), hdl_ref[0], f32)) * softplus(pre_ref[...].astype(f32)) + ex_ref[...]
@@ -272,49 +285,23 @@
         def _(j=j):
             state(j).start()
 
-    pump(1, 0)
+    step(0, 1)
     sx = dot3(s_s[...], x_s[...])
     ol_s[...] = sx[:, :DH]
     p_s[...] = p_s[...] - sx[:, DH:]
     for i in ORDER[:4]:
         d_forward(i)
-    pump(1, 1)
+    step(1, 1)
+    step(2, 1)
+    for n in (8, 9, 10):
+        loaded(n).wait()
+    step(3, 0)
     for i in ORDER[4:]:
         d_forward(i)
-    pump(1, 2)
-    pump(2, 0)
-
-    def experts(slots, start, size, begin):
-        xt = xbuf[pl.ds(start, size), :]
-        total = None
-        for zs in slots:
-            both = dg(xt, gu[zs].reshape(4 * SH, W), 1, 1)
-            g, u = both[:, : 2 * SH], both[:, 2 * SH :]
-            h = (g * sigmoid(g) * u).astype(bf16)
-            part = dg(h, dw[zs].reshape(2 * SH, W))
-            total = part if total is None else total + part
-        return total if begin else acc[pl.ds(start, size), :] + total
-
-    MT = 256
-
-    def group(s):
-        for n in ((0,) if s == 0 else (s, 3 + s)):
-            for piece in range(3):
-                across(n, piece).wait_recv()
-        slots = (z,) if s == 0 else ((z + NZ - s) % NZ, (z + s) % NZ)
-
-        def body(m, carry):
-            start = pl.multiple_of(m * MT, MT)
-            acc[pl.ds(start, MT), :] = experts(slots, start, MT, s == 0)
-            return carry
-
-        lax.fori_loop(0, SEG // MT, body, 0)
-
-    for i in range(1, EP):
-        d_last(i).wait_recv()
-    group(0)
-    pump(2, 1)
-    group(1)
+    step(0, 2)
+    step(1, 2)
+    step(2, 2)
+    step(3, 1)
 
     m_s[...] = jnp.zeros((DH, DH), f32)
     for j in range(EP - 1):
@@ -326,14 +313,11 @@
 
     att = (ol_s[...] + bdot(p_s[...], m_s[...])).astype(bf16)
     att_s[...] = att.reshape(NZ, 2, CAP, DH)
-    loaded(7).wait()
+    loaded(6).wait()
     theirs[...] = dg(att_s[:, 1 - c].reshape(SEG // 2, DH), wo_ref[...]).astype(bf16).reshape(NZ, CAP, W)
     swap = remote(theirs, pbuf, xs.at[0], xs.at[1], tp=mate)
     swap.start()
     mine[...] = dg(att_s[:, c].reshape(SEG // 2, DH), wo_ref[...]).reshape(NZ, CAP, W)
-    pump(2, 2)
-    pump(3, 0)
-    swap.wait_recv()
 
     def grow(zs):
         return mine[zs] + pbuf[zs].astype(f32)
@@ -343,38 +327,31 @@
             return remote(rsp.at[s], rrp.at[s], qs_p.at[s], qr_p.at[s], tp=up)
         return remote(rsm.at[s], rrm.at[s], qs_m.at[s], qr_m.at[s], tp=down)
 
-    rsp[0] = grow((z + 4) % NZ).astype(bf16)
-    rsm[0] = grow((z + NZ - 3) % NZ).astype(bf16)
-    pump(3, 1)
-    group(2)
-    pump(3, 2)
-    sums(0, True).start()
-    sums(0, False).start()
-    group(3)
-    far = (z + 4) % NZ
-    for piece in range(2):
-        pump(4, piece)
-    for n in (7, 8):
-        for piece in range(2):
-            across(n, piece).wait_recv()
-    both = dg(xbuf[...], gu[far].reshape(4 * SH, W), 1, 1)
-    g, u = both[:, : 2 * SH], both[:, 2 * SH :]
-    h_s[...] = (g * sigmoid(g) * u).astype(bf16)
-    pump(4, 2)
-    for n in (7, 8):
-        across(n, 2).wait_recv()
-    for i in (2, 1, 3, 0):
-        start = pl.multiple_of(((y + i) % 4) * (4 * CAP), 4 * CAP)
-        part = pl.ds(start, 4 * CAP)
-        ybuf[part, :] = (acc[part, :] + dg(h_s[part, :], dw[far].reshape(2 * SH, W))).astype(bf16)
-        for n in (2, 0, 1, 3):
-            if i + n:
-                b_first(4 * i + n).start()
-    rbuf[home, :] = ybuf[home, :]
-
-    for i in ORDER[:3]:
-        b_forward(i)
-    for s in range(1, 4):
+    def hidden(zs):
+        both = dg(xbuf[...], gu[zs].reshape(4 * SH, W), 1, 1)
+        g, u = both[:, : 2 * SH], both[:, 2 * SH :]
+        h_s[:, pl.ds(pl.multiple_of(zs * 2 * SH, 2 * SH), 2 * SH)] = (g * sigmoid(g) * u).astype(bf16)
+
+    def group(s):
+        for n in ((0,) if s == 0 else (s, 3 + s)):
+            for piece in range(2):
+                across(n, piece).wait_recv()
+        for zs in (z,) if s == 0 else ((z + NZ - s) % NZ, (z + s) % NZ):
+            hidden(zs)
+
+    def results(n):
+        for m in range(9):
+            across(m, 2 + n).wait_recv()
+        ybuf[n] = dg(h_s[...], dw[n].reshape(16 * SH, COLS)).astype(bf16)
+        for i in ORDER + DIRECT:
+            back[n][0](i).start()
+        rbuf[n, home, :] = ybuf[n, home, :]
+
+    def relay(n):
+        for i in ORDER:
+            back[n][1](i)
+
+    def add(s):
         sums(s - 1, True).wait_recv()
         rsp[s] = (rrp[s - 1].astype(f32) + grow((z + 4 - s) % NZ)).astype(bf16)
         sums(s, True).start()
@@ -382,8 +359,52 @@
             sums(s - 1, False).wait_recv()
             rsm[s] = (rrm[s - 1].astype(f32) + grow((z + NZ - 3 + s) % NZ)).astype(bf16)
             sums(s, False).start()
-        for i in ORDER[1 + 2 * s : 3 + 2 * s]:
-            b_forward(i)
+
+    step(0, 3)
+    for i in range(1, EP):
+        d_last(i).wait_recv()
+    group(0)
+    group(1)
+    step(1, 3)
+    step(2, 3)
+    group(2)
+    step(4, 0)
+    step(3, 2)
+    step(5, 0)
+    swap.wait_recv()
+    rsp[0] = grow((z + 4) % NZ).astype(bf16)
+    rsm[0] = grow((z + NZ - 3) % NZ).astype(bf16)
+    group(3)
+    finish(0)
+    finish(1)
+    finish(2)
+    step(4, 1)
+    for n in (7, 8):
+        for piece in range(2):
+            across(n, piece).wait_recv()
+    hidden((z + 4) % NZ)
+    step(3, 3)
+    results(0)
+    step(5, 1)
+    step(4, 2)
+    finish(3)
+    step(5, 2)
+    results(1)
+    step(4, 3)
+    relay(0)
+    step(5, 3)
+    finish(4)
+    sums(0, True).start()
+    sums(0, False).start()
+    results(2)
+    relay(1)
+    finish(5)
+    results(3)
+    add(1)
+    relay(2)
+    add(2)
+    relay(3)
+    add(3)
     sums(2, False).wait_recv()
     sums(3, True).wait_recv()
     o1_ref[...] = (grow(z) + rrp[3].astype(f32) + rrm[2].astype(f32)).astype(bf16)
@@ -391,22 +412,25 @@
     lead = sigmoid(eld_ref[...])
     w1 = jnp.sum(jnp.where(eye, grw_ref[...] * lead, 0.0), axis=1, keepdims=True)
     w2 = jnp.sum(jnp.where(eye, grw_ref[...] * (1.0 - lead), 0.0), axis=1, keepdims=True)
-    for i in range(1, EP):
-        b_last(i).wait_recv()
-    o2_ref[...] = (w1 * dg(pick1, rbuf[...]) + w2 * dg(pick2, rbuf[...])).astype(bf16)
+    for n in range(CHUNKS):
+        for i in range(1, EP):
+            back[n][2](i).wait_recv()
+        mixed = w1 * dg(pick1, rbuf[n]) + w2 * dg(pick2, rbuf[n])
+        o2_ref[:, n * COLS : (n + 1) * COLS] = mixed.astype(bf16)
 
     for s in range(4):
-        for piece in range(3):
+        for piece in range(PIECES):
             ring(s, piece, True).wait_send()
             ring(s, piece, False).wait_send()
         sums(s, True).wait_send()
         if s < 3:
             sums(s, False).wait_send()
     for n in range(9):
-        for piece in range(3):
+        for piece in range(PIECES):
             across(n, piece).wait_send()
     d_drain()
-    b_drain()
+    for n in range(CHUNKS):
+        back[n][3]()
     swap.wait_send()
     for j in range(1, EP):
 
@@ -420,16 +444,17 @@
     dma = pltpu.SemaphoreType.DMA
     scratch = [
         V((SEG, DH), bf16), V((SEG, DH), bf16), V((SEG, DH), bf16), V((DH, W), bf16), V((TOK, W), bf16),
-        V((NZ, 2, 2, SH, W), bf16), V((NZ, 2, SH, W), bf16),
-        V((SLOTS, W), bf16), V((SLOTS, W), bf16), V((SLOTS, W), bf16), V((SLOTS, W), bf16), V((SLOTS, W), f32),
-        V((7, CAP, W), bf16), V((7, CAP, W), bf16), V((SLOTS, 2 * SH), bf16),
+        V((NZ, 2, 2, SH, W), bf16), V((CHUNKS, NZ, 2, SH, COLS), bf16),
+        V((SLOTS, W), bf16), V((SLOTS, W), bf16), V((CHUNKS, SLOTS, COLS), bf16), V((CHUNKS, SLOTS, COLS), bf16),
+        V((7, CAP, W), bf16), V((CHUNKS, 7, CAP, COLS), bf16), V((SLOTS, 16 * SH), bf16),
         V((SEG, SEG), f32), V((SEG, SEG), f32), V((SEG, 2 * DH), f32), V((SEG, DH), f32), V((SEG, DH), f32),
         V((DH, DH), f32), V((DH, 2 * DH), bf16), V((EP, DH, 2 * DH), bf16), V((NZ, 2, CAP, DH), bf16),
         V((NZ, CAP, W), f32), V((NZ, CAP, W), bf16), V((NZ, CAP, W), bf16),
         V((4, CAP, W), bf16), V((3, CAP, W), bf16), V((4, CAP, W), bf16), V((3, CAP, W), bf16),
-        dma((4, 3)), dma((4, 3)), dma((4, 3)), dma((4, 3)), dma((9, 3)), dma((9, 3)),
-        dma((EP,)), dma((EP,)), dma((7,)), dma((7,)), dma((EP,)), dma((EP,)), dma((7,)), dma((7,)),
-        dma((EP,)), dma((EP,)), dma((2,)), dma((4,)), dma((4,)), dma((3,)), dma((3,)), dma((8,)),
+        dma((4, PIECES)), dma((4, PIECES)), dma((4, PIECES)), dma((4, PIECES)), dma((9, PIECES)), dma((9, PIECES)),
+        dma((EP,)), dma((EP,)), dma((7,)), dma((7,)),
+        dma((CHUNKS, EP)), dma((CHUNKS, EP)), dma((CHUNKS, 7)), dma((CHUNKS, 7)),
+        dma((EP,)), dma((EP,)), dma((2,)), dma((4,)), dma((4,)), dma((3,)), dma((3,)), dma((11,)),
     ]
     vm = pl.BlockSpec(memory_space=pltpu.VMEM)
     hbm = pl.BlockSpec(memory_space=pl.ANY)

time: 113 us -> 103 us (0.912)
  Pallas kernels: 112 us -> 102 us
    pallas_call x1, Pallas kernels: 110 us -> 99.6 us  [shards(): pl.pallas_call(kernel, name='mixer_and_experts', out_shape=(jax.ShapeDtyp...]
where the time goes in v3:
time: 103 us
  Pallas kernels  102 us (99%)
  between operations  1.29 us (1%)
    pallas_call x1, Pallas kernels, shards(): pl.pallas_call(kernel, name='mixer_and_experts', out_shape=(jax.ShapeDtyp...  99.6 us

profile of v3, /device:TPU:1, one launch (start us, length us, event | category | flops | bytes accessed | tf_op | source)
XLA Modules:
  0.0 102.9 jit_solution(7844939001130960491)
XLA Ops:
  1.3 99.6 %mixer_and_experts.1 = (bf16[32,2048]{1,0:T(8,128)(2,1)}, bf16[128,2048]{1,0:T(8,128)(2,1)}) custom-call(bf16[512,128]{1,0:T(8,128)(2,1)} %q_hbm.1, bf16[512,128]{1,0:T(8,128)(2,1)} %k_hbm.1, bf16[512,128]{1,0:T(8,128)(2,1)} %v_hbm.1, bf16[1,512]{1,0:T(2,128)(2,1)} %lg_ref.1, bf16[1,512]{1,0:T(2,128)(2,1)} %pre_ref.1, f32[1]{0:T(128)S(6)} %copy.18.hdl_ref, ...), custom_call_target="tpu_custom_call" | custom-call | tf_op jit(solution)/shard_map/mixer_and_experts/pallas_call | solution.py:461
  100.9 2.0 %hand_over.1 = (bf16[32,2048]{1,0:T(8,128)(2,1)}, bf16[128,2048]{1,0:T(8,128)(2,1)}) custom-call(bf16[32,2048]{1,0:T(8,128)(2,1)} %get-tuple-element.4.a_ref, bf16[128,2048]{1,0:T(8,128)(2,1)} %get-tuple-element.5.b_ref), custom_call_target="tpu_custom_call" | custom-call | tf_op jit(solution)/shard_map/hand_over/pallas_call | solution.py:475

commit v4 on v3

--- a/solution.py
+++ b/solution.py
@@ -63,15 +63,15 @@
 
 
 def kernel(
-    q_hbm, k_hbm, v_hbm, lg_ref, pre_ref, hdl_ref, ex_ref, wo_hbm,
-    tok_hbm, sc_ref, ch_ref, grw_ref, eld_ref, wg_hbm, wu_hbm, wd_hbm,
+    q_hbm, k_hbm, v_hbm, lg_hbm, pre_hbm, hdl_hbm, ex_hbm, wo_hbm,
+    tok_hbm, sc_hbm, ch_hbm, grw_hbm, eld_hbm, wg_hbm, wu_hbm, wd_hbm,
     o1_ref, o2_ref,
-    q_ref, k_ref, v_ref, wo_ref, tok_ref,
+    q_ref, k_ref, v_ref, wo_ref, tok_ref, lg_ref, pre_ref, hdl_ref, ex_ref, sc_ref, ch_ref, grw_ref, eld_ref,
     gu, dw, obuf, xbuf, ybuf, rbuf, dhop, bhop, h_s,
     a_s, s_s, x_s, ol_s, p_s, m_s, st_own, st_all, att_s,
     mine, theirs, pbuf, rrp, rrm, rsp, rsm,
-    sp, rp, sm, rm, ps, pr, dsend, drecv, dhs, dhr, bsend, brecv, bhs, bhr,
-    ssend, srecv, xs, qs_p, qr_p, qs_m, qr_m, ins,
+    rs, rr, ps, pr, dsem, dhr, bsem, brecv, bhr,
+    ssend, srecv, xs, qs, qr_p, qr_m, ins,
 ):
     ep = lax.axis_index("ep")
     tp = lax.axis_index("tp")
@@ -88,11 +88,13 @@
         pairs = (
             (wg_hbm.at[0], gu.at[z, 0, c]), (wu_hbm.at[0], gu.at[z, 1, c]),
             (tok_hbm, tok_ref), (k_hbm, k_ref), (q_hbm, q_ref), (v_hbm, v_ref), (wo_hbm, wo_ref),
+            (sc_hbm, sc_ref), (ch_hbm, ch_ref), (lg_hbm, lg_ref), (pre_hbm, pre_ref), (hdl_hbm, hdl_ref),
+            (ex_hbm, ex_ref), (grw_hbm, grw_ref), (eld_hbm, eld_ref),
             *((wd_hbm.at[0, :, pl.ds(n * COLS, COLS)], dw.at[n, z, c]) for n in range(CHUNKS)),
         )
-        return pltpu.make_async_copy(*pairs[n], ins.at[n])
-
-    for n in (0, 1, 7, 2, 3, 4, 5, 8, 9, 10, 6):
+        return pltpu.make_async_copy(*pairs[n], ins.at[(0, *range(14), 14, 15, 15, 15)[n]])
+
+    for n in (0, 1, 15, 2, 7, 8, 3, 4, 5, 9, 10, 11, 12, 13, 14, 16, 17, 18, 6):
         loaded(n).start()
 
     barrier = pltpu.get_barrier_semaphore()
@@ -107,6 +109,9 @@
             src_ref=src, dst_ref=dst, send_sem=send, recv_sem=recv, device_id=where, device_id_type=MESH
         )
 
+    def absorb(like, sem):
+        pltpu.make_async_copy(like, like, sem).wait()
+
     def place(zs, core, piece, rows):
         whole = gu.at[zs, piece, core] if piece < 2 else dw.at[piece - 2, zs, core]
         return whole if rows is None else whole.at[pl.ds(rows, SH // 2)]
@@ -116,8 +121,12 @@
         rows = None if s < 3 else (0 if forward else SH // 2)
         here = place(slot, c, piece, rows)
         if forward:
-            return remote(here, here, sp.at[s, piece], rp.at[s, piece], tp=up)
-        return remote(here, here, sm.at[s, piece], rm.at[s, piece], tp=down)
+            return remote(here, here, rs.at[min(piece // 2, 1)], rr.at[s, piece], tp=up)
+        return remote(here, here, rs.at[min(piece // 2, 1)], rr.at[s, piece], tp=down)
+
+    def arrived(s, piece):
+        like = gu.at[0, 0] if piece < 2 else dw.at[0, 0]
+        absorb(like if s < 3 else like.at[0], rr.at[s, piece])
 
     def across(n, piece):
         if n == 0:
@@ -129,7 +138,8 @@
         else:
             slot, rows = (z + 4) % NZ, (0 if n == 7 else SH // 2)
         here = place(slot, c, piece, rows)
-        return remote(here, here, ps.at[n, piece], pr.at[n, piece], tp=mate)
+        wave = 0 if n == 0 else (n - 1) % 3 + 1 if n < 7 else 4
+        return remote(here, here, ps.at[min(piece // 2, 1)], pr.at[wave if piece < 2 else 3 + piece], tp=mate)
 
     def step(piece, s):
         if s == 0:
@@ -137,25 +147,24 @@
             ring(0, piece, True).start()
             ring(0, piece, False).start()
             return
-        ring(s - 1, piece, True).wait_recv()
+        arrived(s - 1, piece)
         ring(s, piece, True).start()
+        ring(s, piece, False).start()
         across(s, piece).start()
-        ring(s - 1, piece, False).wait_recv()
-        ring(s, piece, False).start()
         across(3 + s, piece).start()
 
     def finish(piece):
-        ring(3, piece, True).wait_recv()
+        arrived(3, piece)
         across(7, piece).start()
-        ring(3, piece, False).wait_recv()
         across(8, piece).start()
 
-    for n in (0, 1, 7):
-        loaded(n).wait()
+    absorb(gu.at[0, :, 0], ins.at[0])
+    loaded(15).wait()
     for piece in range(3):
         step(piece, 0)
 
-    loaded(2).wait()
+    for n in (2, 7, 8):
+        loaded(n).wait()
     wide = tok_ref[...].astype(f32)
     normed = (
         wide * lax.rsqrt(jnp.sum(wide * wide, axis=1, keepdims=True) * (1.0 / W) + EPS) * sc_ref[...]
@@ -180,33 +189,29 @@
             block = src.at[pl.ds(peer(i) * CAP, CAP)]
             if i in RELAY:
                 n = ORDER.index(i)
-                return remote(block, hop.at[n], send.at[i], hrecv.at[n], ep=peer(RELAY[i]))
-            return remote(block, dst.at[pl.ds(ep * CAP, CAP)], send.at[i], recv.at[i], ep=peer(i))
+                return remote(block, hop.at[n], send, hrecv(n), ep=peer(RELAY[i]))
+            return remote(block, dst.at[pl.ds(ep * CAP, CAP)], send, recv, ep=peer(i))
 
         def second_leg(i):
             n = ORDER.index(i)
             origin = peer(minus(0, RELAY[i]))
             there = dst.at[pl.ds(origin * CAP, CAP)]
-            return remote(hop.at[n], there, hsend.at[n], recv.at[i], ep=peer(minus(i, RELAY[i])))
-
-        def last(i):
-            return remote(src.at[pl.ds(0, CAP)], dst.at[pl.ds(0, CAP)], send.at[i], recv.at[i], ep=peer(i))
-
-        def forward(i):
-            first_leg(i).wait_recv()
-            second_leg(i).start()
-
-        def drain():
-            for i in range(1, EP):
-                first_leg(i).wait_send()
-            for i in ORDER:
-                second_leg(i).wait_send()
-
-        return first_leg, forward, last, drain
-
-    d_first, d_forward, d_last, d_drain = route(obuf, xbuf, dhop, dsend, drecv, dhs, dhr)
+            return remote(hop.at[n], there, hsend, recv, ep=peer(minus(i, RELAY[i])))
+
+        def forward(lo, hi):
+            absorb(hop.at[pl.ds(lo, hi - lo)], hrecv(lo))
+            for i in ORDER[lo:hi]:
+                second_leg(i).start()
+
+        return first_leg, forward
+
+    others = pl.ds(0, (EP - 1) * CAP)
+    d_first, d_forward = route(obuf, xbuf, dhop, dsem.at[0], dsem.at[1], dsem.at[2], lambda n: dhr.at[n // 4])
     back = [
-        route(ybuf.at[n], rbuf.at[n], bhop.at[n], bsend.at[n], brecv.at[n], bhs.at[n], bhr.at[n])
+        route(
+            ybuf.at[n], rbuf.at[n], bhop.at[n], bsem.at[0], brecv.at[n], bsem.at[1],
+            lambda m, n=n: bhr.at[n + (m // 4 if n == CHUNKS - 1 else 0)],
+        )
         for n in range(CHUNKS)
     ]
     for i in ORDER + DIRECT:
@@ -214,7 +219,7 @@
     home = pl.ds(pl.multiple_of(ep * CAP, CAP), CAP)
     xbuf[home, :] = obuf[home, :]
 
-    for n in (3, 4, 5):
+    for n in (3, 4, 5, 9, 10, 11, 12):
         loaded(n).wait()
     kb, qb = k_ref[...], q_ref[...]
     ld = -jnp.exp(jnp.full((1, 1), hdl_ref[0], f32)) * softplus(pre_ref[...].astype(f32)) + ex_ref[...]
@@ -289,15 +294,12 @@
     sx = dot3(s_s[...], x_s[...])
     ol_s[...] = sx[:, :DH]
     p_s[...] = p_s[...] - sx[:, DH:]
-    for i in ORDER[:4]:
-        d_forward(i)
+    d_forward(0, 4)
     step(1, 1)
     step(2, 1)
-    for n in (8, 9, 10):
-        loaded(n).wait()
+    absorb(dw.at[pl.ds(1, 3), 0, 0], ins.at[15])
     step(3, 0)
-    for i in ORDER[4:]:
-        d_forward(i)
+    d_forward(4, 7)
     step(0, 2)
     step(1, 2)
     step(2, 2)
@@ -313,124 +315,152 @@
 
     att = (ol_s[...] + bdot(p_s[...], m_s[...])).astype(bf16)
     att_s[...] = att.reshape(NZ, 2, CAP, DH)
-    loaded(6).wait()
+    for n in (6, 13, 14):
+        loaded(n).wait()
     theirs[...] = dg(att_s[:, 1 - c].reshape(SEG // 2, DH), wo_ref[...]).astype(bf16).reshape(NZ, CAP, W)
     swap = remote(theirs, pbuf, xs.at[0], xs.at[1], tp=mate)
     swap.start()
     mine[...] = dg(att_s[:, c].reshape(SEG // 2, DH), wo_ref[...]).reshape(NZ, CAP, W)
 
-    def grow(zs):
-        return mine[zs] + pbuf[zs].astype(f32)
-
-    def sums(s, forward):
+    def grow(zs, k):
+        cols = slice(k * W // 2, (k + 1) * W // 2)
+        return mine[zs, :, cols] + pbuf[zs, :, cols].astype(f32)
+
+    def sums(s, k, forward):
         if forward:
-            return remote(rsp.at[s], rrp.at[s], qs_p.at[s], qr_p.at[s], tp=up)
-        return remote(rsm.at[s], rrm.at[s], qs_m.at[s], qr_m.at[s], tp=down)
+            return remote(rsp.at[s, k], rrp.at[s, k], qs.at[0], qr_p.at[s, k], tp=up)
+        return remote(rsm.at[s, k], rrm.at[s, k], qs.at[1], qr_m.at[s, k], tp=down)
 
     def hidden(zs):
         both = dg(xbuf[...], gu[zs].reshape(4 * SH, W), 1, 1)
         g, u = both[:, : 2 * SH], both[:, 2 * SH :]
         h_s[:, pl.ds(pl.multiple_of(zs * 2 * SH, 2 * SH), 2 * SH)] = (g * sigmoid(g) * u).astype(bf16)
 
+    def crossed(s):
+        absorb(gu.at[0] if 0 < s < 4 else gu.at[0, 0], pr.at[s])
+
     def group(s):
-        for n in ((0,) if s == 0 else (s, 3 + s)):
-            for piece in range(2):
-                across(n, piece).wait_recv()
-        for zs in (z,) if s == 0 else ((z + NZ - s) % NZ, (z + s) % NZ):
+        for zs in {0: (z,), 4: ((z + 4) % NZ,)}.get(s, ((z + NZ - s) % NZ, (z + s) % NZ)):
             hidden(zs)
 
     def results(n):
-        for m in range(9):
-            across(m, 2 + n).wait_recv()
+        absorb(dw.at[n, :, 0], pr.at[5 + n])
         ybuf[n] = dg(h_s[...], dw[n].reshape(16 * SH, COLS)).astype(bf16)
-        for i in ORDER + DIRECT:
+        rbuf[n, home, :] = ybuf[n, home, :]
+
+    def send(n, messages):
+        for i in messages:
             back[n][0](i).start()
-        rbuf[n, home, :] = ybuf[n, home, :]
 
     def relay(n):
-        for i in ORDER:
-            back[n][1](i)
-
-    def add(s):
-        sums(s - 1, True).wait_recv()
-        rsp[s] = (rrp[s - 1].astype(f32) + grow((z + 4 - s) % NZ)).astype(bf16)
-        sums(s, True).start()
+        if n < CHUNKS - 1:
+            back[n][1](0, 7)
+        else:
+            back[n][1](0, 4)
+            back[n][1](4, 7)
+
+    def begin(k):
+        sums(0, k, True).start()
+        sums(0, k, False).start()
+
+    def add(s, k):
+        sums(s - 1, k, True).wait_recv()
+        rsp[s, k] = (rrp[s - 1, k].astype(f32) + grow((z + 4 - s) % NZ, k)).astype(bf16)
+        sums(s, k, True).start()
         if s < 3:
-            sums(s - 1, False).wait_recv()
-            rsm[s] = (rrm[s - 1].astype(f32) + grow((z + NZ - 3 + s) % NZ)).astype(bf16)
-            sums(s, False).start()
+            sums(s - 1, k, False).wait_recv()
+            rsm[s, k] = (rrm[s - 1, k].astype(f32) + grow((z + NZ - 3 + s) % NZ, k)).astype(bf16)
+            sums(s, k, False).start()
+
+    def total(k):
+        sums(2, k, False).wait_recv()
+        sums(3, k, True).wait_recv()
+        o1_ref[:, k * W // 2 : (k + 1) * W // 2] = (
+            grow(z, k) + rrp[3, k].astype(f32) + rrm[2, k].astype(f32)
+        ).astype(bf16)
+
+    lead = sigmoid(eld_ref[...])
+    w1 = jnp.sum(jnp.where(eye, grw_ref[...] * lead, 0.0), axis=1, keepdims=True)
+    w2 = jnp.sum(jnp.where(eye, grw_ref[...] * (1.0 - lead), 0.0), axis=1, keepdims=True)
+
+    def mix(n):
+        absorb(rbuf.at[n, others], brecv.at[n])
+        mixed = w1 * dg(pick1, rbuf[n]) + w2 * dg(pick2, rbuf[n])
+        o2_ref[:, n * COLS : (n + 1) * COLS] = mixed.astype(bf16)
 
     step(0, 3)
-    for i in range(1, EP):
-        d_last(i).wait_recv()
+    absorb(xbuf.at[others], dsem.at[1])
+    crossed(0)
     group(0)
+    crossed(1)
     group(1)
     step(1, 3)
     step(2, 3)
+    step(4, 0)
+    crossed(2)
     group(2)
-    step(4, 0)
     step(3, 2)
     step(5, 0)
     swap.wait_recv()
-    rsp[0] = grow((z + 4) % NZ).astype(bf16)
-    rsm[0] = grow((z + NZ - 3) % NZ).astype(bf16)
+    for k in range(2):
+        rsp[0, k] = grow((z + 4) % NZ, k).astype(bf16)
+        rsm[0, k] = grow((z + NZ - 3) % NZ, k).astype(bf16)
+    crossed(3)
     group(3)
     finish(0)
     finish(1)
     finish(2)
+    crossed(4)
     step(4, 1)
-    for n in (7, 8):
-        for piece in range(2):
-            across(n, piece).wait_recv()
-    hidden((z + 4) % NZ)
+    group(4)
+    results(0)
+    send(0, ORDER + DIRECT)
     step(3, 3)
-    results(0)
     step(5, 1)
     step(4, 2)
+    begin(0)
     finish(3)
     step(5, 2)
     results(1)
+    send(1, ORDER + DIRECT)
     step(4, 3)
+    begin(1)
     relay(0)
     step(5, 3)
+    add(1, 0)
     finish(4)
-    sums(0, True).start()
-    sums(0, False).start()
     results(2)
+    send(2, ORDER)
+    add(1, 1)
     relay(1)
     finish(5)
     results(3)
-    add(1)
+    send(3, ORDER)
+    send(2, DIRECT)
+    send(3, DIRECT)
+    add(2, 0)
+    add(2, 1)
+    mix(0)
     relay(2)
-    add(2)
+    add(3, 0)
     relay(3)
-    add(3)
-    sums(2, False).wait_recv()
-    sums(3, True).wait_recv()
-    o1_ref[...] = (grow(z) + rrp[3].astype(f32) + rrm[2].astype(f32)).astype(bf16)
-
-    lead = sigmoid(eld_ref[...])
-    w1 = jnp.sum(jnp.where(eye, grw_ref[...] * lead, 0.0), axis=1, keepdims=True)
-    w2 = jnp.sum(jnp.where(eye, grw_ref[...] * (1.0 - lead), 0.0), axis=1, keepdims=True)
-    for n in range(CHUNKS):
-        for i in range(1, EP):
-            back[n][2](i).wait_recv()
-        mixed = w1 * dg(pick1, rbuf[n]) + w2 * dg(pick2, rbuf[n])
-        o2_ref[:, n * COLS : (n + 1) * COLS] = mixed.astype(bf16)
-
-    for s in range(4):
-        for piece in range(PIECES):
-            ring(s, piece, True).wait_send()
-            ring(s, piece, False).wait_send()
-        sums(s, True).wait_send()
-        if s < 3:
-            sums(s, False).wait_send()
-    for n in range(9):
-        for piece in range(PIECES):
-            across(n, piece).wait_send()
-    d_drain()
-    for n in range(CHUNKS):
-        back[n][3]()
+    add(3, 1)
+    mix(1)
+    total(0)
+    total(1)
+    mix(2)
+    mix(3)
+
+    absorb(gu.at[pl.ds(0, 7), :, 0], rs.at[0])
+    absorb(dw.at[:, pl.ds(0, 7), 0], rs.at[1])
+    absorb(gu.at[:, :, 0], ps.at[0])
+    absorb(dw.at[:, :, 0], ps.at[1])
+    absorb(obuf.at[others], dsem.at[0])
+    absorb(dhop, dsem.at[2])
+    absorb(ybuf.at[:, others], bsem.at[0])
+    absorb(bhop, bsem.at[1])
+    absorb(rsp, qs.at[0])
+    absorb(rsm, qs.at[1])
     swap.wait_send()
     for j in range(1, EP):
 
@@ -444,25 +474,27 @@
     dma = pltpu.SemaphoreType.DMA
     scratch = [
         V((SEG, DH), bf16), V((SEG, DH), bf16), V((SEG, DH), bf16), V((DH, W), bf16), V((TOK, W), bf16),
+        V((1, SEG), bf16), V((1, SEG), bf16), pltpu.SMEM((1,), f32), V((1, SEG), f32),
+        V((1, W), f32), V((2, TOK), jnp.int32), V((1, TOK), f32), V((1, TOK), f32),
         V((NZ, 2, 2, SH, W), bf16), V((CHUNKS, NZ, 2, SH, COLS), bf16),
         V((SLOTS, W), bf16), V((SLOTS, W), bf16), V((CHUNKS, SLOTS, COLS), bf16), V((CHUNKS, SLOTS, COLS), bf16),
         V((7, CAP, W), bf16), V((CHUNKS, 7, CAP, COLS), bf16), V((SLOTS, 16 * SH), bf16),
         V((SEG, SEG), f32), V((SEG, SEG), f32), V((SEG, 2 * DH), f32), V((SEG, DH), f32), V((SEG, DH), f32),
         V((DH, DH), f32), V((DH, 2 * DH), bf16), V((EP, DH, 2 * DH), bf16), V((NZ, 2, CAP, DH), bf16),
         V((NZ, CAP, W), f32), V((NZ, CAP, W), bf16), V((NZ, CAP, W), bf16),
-        V((4, CAP, W), bf16), V((3, CAP, W), bf16), V((4, CAP, W), bf16), V((3, CAP, W), bf16),
-        dma((4, PIECES)), dma((4, PIECES)), dma((4, PIECES)), dma((4, PIECES)), dma((9, PIECES)), dma((9, PIECES)),
-        dma((EP,)), dma((EP,)), dma((7,)), dma((7,)),
-        dma((CHUNKS, EP)), dma((CHUNKS, EP)), dma((CHUNKS, 7)), dma((CHUNKS, 7)),
-        dma((EP,)), dma((EP,)), dma((2,)), dma((4,)), dma((4,)), dma((3,)), dma((3,)), dma((11,)),
+        V((4, 2, CAP, W // 2), bf16), V((3, 2, CAP, W // 2), bf16),
+        V((4, 2, CAP, W // 2), bf16), V((3, 2, CAP, W // 2), bf16),
+        dma((2,)), dma((4, PIECES)), dma((2,)), dma((5 + CHUNKS,)),
+        dma((3,)), dma((2,)), dma((2,)), dma((CHUNKS,)), dma((CHUNKS + 1,)),
+        dma((EP,)), dma((EP,)), dma((2,)), dma((2,)), dma((4, 2)), dma((3, 2)), dma((16,)),
     ]
     vm = pl.BlockSpec(memory_space=pltpu.VMEM)
     hbm = pl.BlockSpec(memory_space=pl.ANY)
     outs = pl.pallas_call(
         kernel,
         name="mixer_and_experts",
-        out_shape=(jax.ShapeDtypeStruct((CAP, W), bf16), jax.ShapeDtypeStruct((TOK, W), bf16)),
-        in_specs=[hbm, hbm, hbm, vm, vm, pl.BlockSpec(memory_space=pltpu.SMEM), vm, hbm, hbm, vm, vm, vm, vm, hbm, hbm, hbm],
+        out_shape=(V((CAP, W), bf16), V((TOK, W), bf16)),
+        in_specs=[hbm] * 16,
         out_specs=(vm, vm),
         scratch_shapes=scratch,
         compiler_params=pltpu.CompilerParams(
@@ -478,7 +510,7 @@
         out_shape=(jax.ShapeDtypeStruct((CAP, W), bf16), jax.ShapeDtypeStruct((TOK, W), bf16)),
         in_specs=[vm, vm],
         out_specs=(vm, vm),
-        compiler_params=pltpu.CompilerParams(vmem_limit_bytes=60 * 1024 * 1024),
+        compiler_params=pltpu.CompilerParams(vmem_limit_bytes=4 * 1024 * 1024),
     )(*outs)
 
 

time: 103 us -> 95 us (0.922)
  Pallas kernels: 102 us -> 93.6 us
    pallas_call x1, Pallas kernels: 99.6 us -> 92.7 us  [shards(): pl.pallas_call(kernel, name='mixer_and_experts', out_shape=(V((CAP, W), b...]
    pallas_call x1, Pallas kernels: 1.96 us -> 0.88 us  [shards(): pl.pallas_call(hand_over, name='hand_over', out_shape=(jax.ShapeDtypeStru...]
where the time goes in v4:
time: 95 us; the launch traced here: 94.9 us
  Pallas kernels  93.6 us (99%)
  between operations  1.29 us (1%)
    pallas_call x1, Pallas kernels, shards(): pl.pallas_call(kernel, name='mixer_and_experts', out_shape=(V((CAP, W), b...  92.7 us

profile of v4, /device:TPU:1, one launch (start us, length us, event | category | flops | bytes accessed | tf_op | source)
XLA Modules:
  0.0 94.9 jit_solution(12955772521689424140)
XLA Ops:
  1.3 92.7 %mixer_and_experts.1 = (bf16[32,2048]{1,0:T(8,128)(2,1)S(1)}, bf16[128,2048]{1,0:T(8,128)(2,1)S(1)}) custom-call(bf16[512,128]{1,0:T(8,128)(2,1)} %q_hbm.1, bf16[512,128]{1,0:T(8,128)(2,1)} %k_hbm.1, bf16[512,128]{1,0:T(8,128)(2,1)} %v_hbm.1, bf16[1,512]{1,0:T(2,128)(2,1)} %lg_hbm.1, bf16[1,512]{1,0:T(2,128)(2,1)} %pre_hbm.1, f32[1]{0:T(128)S(6)} %copy.18.hdl_hbm, ...), custom_call_target="tpu_custom_call" | custom-call | tf_op jit(solution)/shard_map/mixer_and_experts/pallas_call | solution.py:493
  94.0 0.9 hand_over.1

commit v5 on v4

--- a/solution.py
+++ b/solution.py
@@ -22,6 +22,7 @@
 COLS = W // CHUNKS
 PIECES = 2 + CHUNKS
 SLOTS = EXPERTS * CAP
+ROWS = (slice(0, SLOTS // 2), slice(SLOTS // 2, SLOTS))
 RELAY = {10: 15, 8: 4, 9: 13, 11: 7, 6: 7, 14: 13, 2: 1}
 ORDER = list(RELAY)
 DIRECT = [i for i in range(1, 16) if i not in RELAY]
@@ -332,9 +333,11 @@
         return remote(rsm.at[s, k], rrm.at[s, k], qs.at[1], qr_m.at[s, k], tp=down)
 
     def hidden(zs):
-        both = dg(xbuf[...], gu[zs].reshape(4 * SH, W), 1, 1)
-        g, u = both[:, : 2 * SH], both[:, 2 * SH :]
-        h_s[:, pl.ds(pl.multiple_of(zs * 2 * SH, 2 * SH), 2 * SH)] = (g * sigmoid(g) * u).astype(bf16)
+        weights = gu[zs].reshape(4 * SH, W)
+        both = [dg(xbuf[rows, :], weights, 1, 1) for rows in ROWS]
+        for rows, b in zip(ROWS, both):
+            g, u = b[:, : 2 * SH], b[:, 2 * SH :]
+            h_s[rows, pl.ds(pl.multiple_of(zs * 2 * SH, 2 * SH), 2 * SH)] = (g * sigmoid(g) * u).astype(bf16)
 
     def crossed(s):
         absorb(gu.at[0] if 0 < s < 4 else gu.at[0, 0], pr.at[s])
@@ -410,11 +413,22 @@
     finish(0)
     finish(1)
     finish(2)
-    crossed(4)
-    step(4, 1)
-    group(4)
-    results(0)
-    send(0, ORDER + DIRECT)
+    @pl.when(c == 0)
+    def _():
+        crossed(4)
+        group(4)
+        results(0)
+        send(0, ORDER + DIRECT)
+        step(4, 1)
+
+    @pl.when(c == 1)
+    def _():
+        step(4, 1)
+        crossed(4)
+        group(4)
+        results(0)
+        send(0, ORDER + DIRECT)
+
     step(3, 3)
     step(5, 1)
     step(4, 2)
@@ -431,24 +445,24 @@
     finish(4)
     results(2)
     send(2, ORDER)
+    relay(1)
+    send(2, DIRECT)
     add(1, 1)
-    relay(1)
     finish(5)
     results(3)
     send(3, ORDER)
-    send(2, DIRECT)
+    add(2, 0)
+    relay(2)
     send(3, DIRECT)
-    add(2, 0)
     add(2, 1)
     mix(0)
-    relay(2)
+    mix(1)
     add(3, 0)
     relay(3)
     add(3, 1)
-    mix(1)
+    mix(2)
     total(0)
     total(1)
-    mix(2)
     mix(3)
 
     absorb(gu.at[pl.ds(0, 7), :, 0], rs.at[0])

time: 95 us -> 94.8 us (level)
  no operation moved by 1% of the time
where the time goes in v5:
time: 94.8 us; the launch traced here: 94.7 us
  Pallas kernels  93.4 us (99%)
  between operations  1.29 us (1%)
    pallas_call x1, Pallas kernels, shards(): pl.pallas_call(kernel, name='mixer_and_experts', out_shape=(V((CAP, W), b...  92.5 us

profile of v5, /device:TPU:1, one launch (start us, length us, event | category | flops | bytes accessed | tf_op | source)
XLA Modules:
  0.0 94.7 jit_solution(12048381270704296406)
XLA Ops:
  1.3 92.5 %mixer_and_experts.1 = (bf16[32,2048]{1,0:T(8,128)(2,1)S(1)}, bf16[128,2048]{1,0:T(8,128)(2,1)S(1)}) custom-call(bf16[512,128]{1,0:T(8,128)(2,1)} %q_hbm.1, bf16[512,128]{1,0:T(8,128)(2,1)} %k_hbm.1, bf16[512,128]{1,0:T(8,128)(2,1)} %v_hbm.1, bf16[1,512]{1,0:T(2,128)(2,1)} %lg_hbm.1, bf16[1,512]{1,0:T(2,128)(2,1)} %pre_hbm.1, f32[1]{0:T(128)S(6)} %copy.18.hdl_hbm, ...), custom_call_target="tpu_custom_call" | custom-call | tf_op jit(solution)/shard_map/mixer_and_experts/pallas_call | solution.py:507
  93.8 0.9 hand_over.1

commit v6 on v5

--- a/solution.py
+++ b/solution.py
@@ -95,14 +95,13 @@
         )
         return pltpu.make_async_copy(*pairs[n], ins.at[(0, *range(14), 14, 15, 15, 15)[n]])
 
-    for n in (0, 1, 15, 2, 7, 8, 3, 4, 5, 9, 10, 11, 12, 13, 14, 16, 17, 18, 6):
-        loaded(n).start()
-
     barrier = pltpu.get_barrier_semaphore()
-    for i in range(1, EP):
+    for i in ORDER + DIRECT:
         pl.semaphore_signal(barrier, inc=1, device_id={"ep": peer(i)}, device_id_type=MESH)
     for t in (up, down, mate):
         pl.semaphore_signal(barrier, inc=1, device_id={"tp": t}, device_id_type=MESH)
+    for n in (0, 1, 15, 2, 7, 8, 3, 4, 5, 9, 10, 11, 12, 13, 14, 16, 17, 18, 6):
+        loaded(n).start()
     pl.semaphore_wait(barrier, EP - 1 + 3)
 
     def remote(src, dst, send, recv, **where):
@@ -412,17 +411,18 @@
     group(3)
     finish(0)
     finish(1)
-    finish(2)
     @pl.when(c == 0)
     def _():
         crossed(4)
         group(4)
+        finish(2)
         results(0)
         send(0, ORDER + DIRECT)
         step(4, 1)
 
     @pl.when(c == 1)
     def _():
+        finish(2)
         step(4, 1)
         crossed(4)
         group(4)

time: 94.8 us -> 94.4 us (level)
  no operation moved by 1% of the time
where the time goes in v6:
time: 94.4 us
  Pallas kernels  93.1 us (99%)
  between operations  1.29 us (1%)
    pallas_call x1, Pallas kernels, shards(): pl.pallas_call(kernel, name='mixer_and_experts', out_shape=(V((CAP, W), b...  92.2 us

profile of v6, /device:TPU:1, one launch (start us, length us, event | category | flops | bytes accessed | tf_op | source)
XLA Modules:
  0.0 94.4 jit_solution(74002338393178715)
XLA Ops:
  1.3 92.2 %mixer_and_experts.1 = (bf16[32,2048]{1,0:T(8,128)(2,1)S(1)}, bf16[128,2048]{1,0:T(8,128)(2,1)S(1)}) custom-call(bf16[512,128]{1,0:T(8,128)(2,1)} %q_hbm.1, bf16[512,128]{1,0:T(8,128)(2,1)} %k_hbm.1, bf16[512,128]{1,0:T(8,128)(2,1)} %v_hbm.1, bf16[1,512]{1,0:T(2,128)(2,1)} %lg_hbm.1, bf16[1,512]{1,0:T(2,128)(2,1)} %pre_hbm.1, f32[1]{0:T(128)S(6)} %copy.18.hdl_hbm, ...), custom_call_target="tpu_custom_call" | custom-call | tf_op jit(solution)/shard_map/mixer_and_experts/pallas_call | solution.py:507
  93.5 0.9 hand_over.1

commit v7 on v6

--- a/solution.py
+++ b/solution.py
@@ -347,7 +347,14 @@
 
     def results(n):
         absorb(dw.at[n, :, 0], pr.at[5 + n])
-        ybuf[n] = dg(h_s[...], dw[n].reshape(16 * SH, COLS)).astype(bf16)
+        weights = dw[n].reshape(16 * SH, COLS)
+        block = 4 * CAP
+        for pair in ((2, 1), (3, 0)):
+            rows = [pl.ds(pl.multiple_of(((y + d) % 4) * block, block), block) for d in pair]
+            both = dg(jnp.concatenate([h_s[r, :] for r in rows], axis=0), weights).astype(bf16)
+            for k, r in enumerate(rows):
+                ybuf[n, r, :] = both[k * block : (k + 1) * block]
+            send(n, [i for i in ORDER if i // 4 in pair])
         rbuf[n, home, :] = ybuf[n, home, :]
 
     def send(n, messages):
@@ -417,7 +424,7 @@
         group(4)
         finish(2)
         results(0)
-        send(0, ORDER + DIRECT)
+        send(0, DIRECT)
         step(4, 1)
 
     @pl.when(c == 1)
@@ -427,7 +434,7 @@
         crossed(4)
         group(4)
         results(0)
-        send(0, ORDER + DIRECT)
+        send(0, DIRECT)
 
     step(3, 3)
     step(5, 1)
@@ -436,7 +443,7 @@
     finish(3)
     step(5, 2)
     results(1)
-    send(1, ORDER + DIRECT)
+    send(1, DIRECT)
     step(4, 3)
     begin(1)
     relay(0)
@@ -444,13 +451,11 @@
     add(1, 0)
     finish(4)
     results(2)
-    send(2, ORDER)
     relay(1)
     send(2, DIRECT)
     add(1, 1)
     finish(5)
     results(3)
-    send(3, ORDER)
     add(2, 0)
     relay(2)
     send(3, DIRECT)

time: 94.4 us -> 94.4 us (level)
  no operation moved by 1% of the time
where the time goes in v7:
time: 94.4 us; the launch traced here: 94.3 us
  Pallas kernels  93 us (99%)
  between operations  1.29 us (1%)
    pallas_call x1, Pallas kernels, shards(): pl.pallas_call(kernel, name='mixer_and_experts', out_shape=(V((CAP, W), b...  92.1 us

profile of v7, /device:TPU:1, one launch (start us, length us, event | category | flops | bytes accessed | tf_op | source)
XLA Modules:
  0.0 94.3 jit_solution(12941751568366744070)
XLA Ops:
  1.3 92.1 %mixer_and_experts.1 = (bf16[32,2048]{1,0:T(8,128)(2,1)S(1)}, bf16[128,2048]{1,0:T(8,128)(2,1)S(1)}) custom-call(bf16[512,128]{1,0:T(8,128)(2,1)} %q_hbm.1, bf16[512,128]{1,0:T(8,128)(2,1)} %k_hbm.1, bf16[512,128]{1,0:T(8,128)(2,1)} %v_hbm.1, bf16[1,512]{1,0:T(2,128)(2,1)} %lg_hbm.1, bf16[1,512]{1,0:T(2,128)(2,1)} %pre_hbm.1, f32[1]{0:T(128)S(6)} %copy.18.hdl_hbm, ...), custom_call_target="tpu_custom_call" | custom-call | tf_op jit(solution)/shard_map/mixer_and_experts/pallas_call | solution.py:512
  93.4 0.9 hand_over.1

commit v8 on v7

--- a/solution.py
+++ b/solution.py
@@ -452,10 +452,10 @@
     finish(4)
     results(2)
     relay(1)
-    send(2, DIRECT)
     add(1, 1)
     finish(5)
     results(3)
+    send(2, DIRECT)
     add(2, 0)
     relay(2)
     send(3, DIRECT)

time: 94.4 us -> 94.2 us (level)
  no operation moved by 1% of the time
where the time goes in v8:
time: 94.2 us; the launch traced here: 94.1 us
  Pallas kernels  92.8 us (99%)
  between operations  1.29 us (1%)
    pallas_call x1, Pallas kernels, shards(): pl.pallas_call(kernel, name='mixer_and_experts', out_shape=(V((CAP, W), b...  91.9 us

profile of v8, /device:TPU:1, one launch (start us, length us, event | category | flops | bytes accessed | tf_op | source)
XLA Modules:
  0.0 94.1 jit_solution(12101734928469249186)
XLA Ops:
  1.3 91.9 %mixer_and_experts.1 = (bf16[32,2048]{1,0:T(8,128)(2,1)S(1)}, bf16[128,2048]{1,0:T(8,128)(2,1)S(1)}) custom-call(bf16[512,128]{1,0:T(8,128)(2,1)} %q_hbm.1, bf16[512,128]{1,0:T(8,128)(2,1)} %k_hbm.1, bf16[512,128]{1,0:T(8,128)(2,1)} %v_hbm.1, bf16[1,512]{1,0:T(2,128)(2,1)} %lg_hbm.1, bf16[1,512]{1,0:T(2,128)(2,1)} %pre_hbm.1, f32[1]{0:T(128)S(6)} %copy.18.hdl_hbm, ...), custom_call_target="tpu_custom_call" | custom-call | tf_op jit(solution)/shard_map/mixer_and_experts/pallas_call | solution.py:512
  93.2 0.9 hand_over.1
